TPU v7x, 256 devices: a whole 4x4x8 slice. The times are simulated.
256 devices in a mesh: ep: 32 (over z, x), tp: 8 (over y, core).
Axes of the slice: x: 4, y: 4, z: 8, core: 2. Of those that a mesh axis runs over, the one named last changes fastest.
Arguments:
- tokens: bfloat16 [512, 1024], P('ep'), may hold values from -6 to 6
- norm_gain: float32 [1024], replicated, may hold values from 0.1 to 1.9
- routing: int32 [512, 2], P('ep'), may hold values from 0 to 31, all different within a row; in each aligned block of 16 rows (0 to 15, 16 to 31, ...) at most 8 rows name the same one
- route_weight: float32 [512, 2], P('ep'), may hold values from 0.1 to 1
- w_gate: bfloat16 [32, 1024, 3584], P('ep', None, 'tp'), may hold values from -0.1875 to 0.1875
- w_up: bfloat16 [32, 1024, 3584], P('ep', None, 'tp'), may hold values from -0.1875 to 0.1875
- w_down: bfloat16 [32, 3584, 1024], P('ep', 'tp'), may hold values from -0.09375 to 0.09375
Outputs:
- mixed: bfloat16 [512, 1024], P('ep', 'tp')
Inputs may be any that keep to these rules, and one draw needn't show every extreme that they name: `routing`: each row names 2 different experts of 0 to 31; among the 16 tokens of one index of ep no expert is named more than 8 times, and in some draws' blocks exactly 8 times.
All inputs are finite; a program needn't handle non-finite values.
Results may differ from a plain program's by a relative error of at most 0.0022.
Values may be sent and summed in bfloat16 or wider, within the bound.
A program may use at most 64 MiB of HBM per device.

v0:
```python
import functools

import jax
import jax.numpy as jnp
from jax import lax
from jax.experimental import pallas as pl
from jax.experimental.pallas import tpu as pltpu
from jax.sharding import PartitionSpec as P

CAP = 8
MESH = pl.DeviceIdType.MESH

norm_eps = 1e-06


def each(low, high, step):
    if high - low <= 8:
        for index in range(low, high):
            step(index)
    else:
        lax.fori_loop(low, high, lambda index, carry: (step(index), carry)[1], 0)


def kernel(groups, shares, tokens_hbm, gain_hbm, routing_hbm, route_weight_hbm, gate_hbm, up_hbm, down_hbm, mixed,
           tokens, gain, routing, route_weight,
           gate, up, down, outgoing, incoming, lent, borrowed, partial, arrived, load_sem, send_sem, recv_sem):
    ep, tp = lax.axis_index("ep"), lax.axis_index("tp")
    width = tokens.shape[1]
    part = mixed.shape[1]
    slots = groups * CAP
    rows = shares // 2
    row, core = tp // 2, lax.rem(tp, 2)

    def toward(q):
        return lax.rem(row + q // 2, rows) * 2 + lax.rem(core + q % 2, 2)

    def far_first(step):
        return step + (1 - 2 * ep // groups) * (groups - 1 - 2 * step)

    pairs = ((tokens_hbm, tokens), (gain_hbm, gain), (routing_hbm, routing), (route_weight_hbm, route_weight),
             (gate_hbm.at[0], gate), (up_hbm.at[0], up), (down_hbm.at[0], down))
    loads = [pltpu.make_async_copy(source, target, load_sem.at[i]) for i, (source, target) in enumerate(pairs)]
    for load in loads:
        load.start()

    barrier = pltpu.get_barrier_semaphore()

    def greet(d):
        pl.semaphore_signal(barrier, inc=1, device_id=(lax.rem(ep + d, groups), tp), device_id_type=MESH)
    each(1, groups, greet)
    for q in range(1, shares):
        pl.semaphore_signal(barrier, inc=1, device_id=(ep, toward(q)), device_id_type=MESH)

    count = tokens.shape[0]
    line = lax.broadcasted_iota(jnp.int32, (slots, count), 0)
    expert = lax.rem(line // CAP + ep, groups)
    member = jnp.zeros((slots, count), jnp.float32)
    weight = jnp.zeros((slots, count), jnp.float32)
    loads[2].wait()
    loads[3].wait()
    for k in range(routing.shape[0]):
        named = routing[k:k + 1, :] == expert
        member = jnp.where(named, 1.0, member)
        weight = jnp.where(named, route_weight[k:k + 1, :], weight)
    earlier = lax.broadcasted_iota(jnp.int32, (count, count), 0) < lax.broadcasted_iota(jnp.int32, (count, count), 1)
    before = jnp.dot(member.astype(jnp.bfloat16), jnp.where(earlier, 1.0, 0.0).astype(jnp.bfloat16),
                     preferred_element_type=jnp.float32)
    placed = jnp.where(before == lax.rem(line, CAP).astype(jnp.float32), member, 0.0)
    weight = jnp.transpose(weight * placed)

    loads[0].wait()
    loads[1].wait()
    values = tokens[...].astype(jnp.float32)
    scale = lax.rsqrt(jnp.mean(values * values, axis=-1, keepdims=True) + norm_eps)
    normed = (values * scale * gain[...]).astype(jnp.bfloat16)
    sent = jnp.dot(placed.astype(jnp.bfloat16), normed, preferred_element_type=jnp.float32)
    outgoing[...] = sent.reshape(groups, CAP, width).astype(jnp.bfloat16)

    pl.semaphore_wait(barrier, groups + shares - 2)

    def dispatch(d):
        pltpu.make_async_remote_copy(
            src_ref=outgoing.at[d], dst_ref=incoming.at[d], send_sem=send_sem.at[0], recv_sem=recv_sem.at[0],
            device_id=(lax.rem(ep + d, groups), tp), device_id_type=MESH).start()
    each(1, groups, dispatch)
    incoming[0] = outgoing[0]

    loads[4].wait()
    loads[5].wait()
    others = pl.ds(1, groups - 1)
    pltpu.make_async_copy(incoming.at[others], incoming.at[others], recv_sem.at[0]).wait()

    x = incoming[...].astype(jnp.float32).reshape(slots, width).astype(jnp.bfloat16)
    gate_act = jnp.dot(x, gate[...], preferred_element_type=jnp.float32)
    up_act = jnp.dot(x, up[...], preferred_element_type=jnp.float32)
    hidden = (gate_act / (1.0 + jnp.exp(-gate_act)) * up_act).astype(jnp.bfloat16)
    loads[6].wait()

    def block_of(q, side):
        columns = pl.ds(pl.multiple_of((lax.rem(row + q, rows) * 2 + side) * part, part), part)
        return jnp.dot(hidden, down[:, columns], preferred_element_type=jnp.float32)

    def give(place, q):
        def to(step):
            target = far_first(step)

            def copy():
                d = lax.rem(ep - target + groups, groups)
                pltpu.make_async_remote_copy(
                    src_ref=partial.at[place * groups + d], dst_ref=arrived.at[place * groups + d],
                    send_sem=send_sem.at[1], recv_sem=recv_sem.at[1],
                    device_id=(target, toward(q)), device_id_type=MESH).start()
            if q == 0:
                pl.when(target != ep)(copy)
            else:
                copy()
        each(0, groups, to)

    for q in range(2, shares):
        block = block_of(q // 2, lax.rem(core + q, 2))
        partial[(q - 1) * groups:q * groups] = block.reshape(groups, CAP, part)
        give(q - 1, q)

    lent[...] = block_of(0, 1 - core)
    lend = pltpu.make_async_remote_copy(
        src_ref=lent, dst_ref=borrowed, send_sem=send_sem.at[2], recv_sem=recv_sem.at[2],
        device_id=(ep, toward(1)), device_id_type=MESH)
    lend.start()
    block = block_of(0, core)
    lend.wait_recv()
    partial[0:groups] = (block + borrowed[...]).reshape(groups, CAP, part)
    give(0, 0)
    arrived[0] = partial[0]

    rest = pl.ds(1, groups * (shares - 1) - 1)
    pltpu.make_async_copy(arrived.at[rest], arrived.at[rest], recv_sem.at[1]).wait()
    total = arrived[0:groups]
    for q in range(1, shares - 1):
        total = total + arrived[q * groups:(q + 1) * groups]
    out = jnp.dot(weight, total.reshape(slots, part), precision=lax.Precision.HIGHEST,
                  preferred_element_type=jnp.float32)
    mixed[...] = out.astype(mixed.dtype)
    pltpu.make_async_copy(outgoing.at[others], outgoing.at[others], send_sem.at[0]).wait()
    pltpu.make_async_copy(partial.at[rest], partial.at[rest], send_sem.at[1]).wait()
    lend.wait_send()


def solution(mesh):
    groups, shares = mesh.shape["ep"], mesh.shape["tp"]

    def local(tokens, norm_gain, routing, route_weight, w_gate, w_up, w_down):
        count, width = tokens.shape
        part = width // shares
        vmem = pl.BlockSpec(memory_space=pltpu.VMEM)
        hbm = pl.BlockSpec(memory_space=pltpu.HBM)
        return pl.pallas_call(
            functools.partial(kernel, groups, shares),
            out_shape=jax.ShapeDtypeStruct((count, part), jnp.bfloat16),
            in_specs=[hbm] * 7,
            out_specs=vmem,
            scratch_shapes=[
                pltpu.VMEM((count, width), tokens.dtype),
                pltpu.VMEM((1, width), norm_gain.dtype),
                pltpu.VMEM(routing.shape[::-1], routing.dtype),
                pltpu.VMEM(route_weight.shape[::-1], route_weight.dtype),
                pltpu.VMEM(w_gate.shape[1:], jnp.bfloat16),
                pltpu.VMEM(w_up.shape[1:], jnp.bfloat16),
                pltpu.VMEM(w_down.shape[1:], jnp.bfloat16),
                pltpu.VMEM((groups, CAP, width), jnp.bfloat16),
                pltpu.VMEM((groups, CAP, width), jnp.bfloat16),
                pltpu.VMEM((groups * CAP, part), jnp.float32),
                pltpu.VMEM((groups * CAP, part), jnp.float32),
                pltpu.VMEM((groups * (shares - 1), CAP, part), jnp.float32),
                pltpu.VMEM((groups * (shares - 1), CAP, part), jnp.float32),
                pltpu.SemaphoreType.DMA((7,)),
                pltpu.SemaphoreType.DMA((3,)),
                pltpu.SemaphoreType.DMA((3,)),
            ],
            compiler_params=pltpu.CompilerParams(collective_id=0, has_side_effects=True,
                                                 vmem_limit_bytes=67043328),
            name="experts",
        )(tokens, norm_gain.reshape(1, width), routing.T, route_weight.T, w_gate, w_up, w_down)

    in_specs = (
        P("ep", None),
        P(),
        P("ep", None),
        P("ep", None),
        P("ep", None, "tp"),
        P("ep", None, "tp"),
        P("ep", "tp", None),
    )
    return jax.shard_map(local, mesh=mesh, in_specs=in_specs, out_specs=P("ep", "tp"), check_vma=False)
```

profile of v0, /device:TPU:1, one launch (start us, length us, event | category | flops | bytes accessed | tf_op | source)
XLA Modules:
  0.0 54.7 jit_solution(15816715380519008578)
XLA Ops:
  0.0 0.0 copy-start
  0.0 2.3 %copy.8.gate_hbm = bf16[1,1024,448]{2,1,0:T(8,128)(2,1)} copy(bf16[1,1024,448]{1,2,0:T(8,128)(2,1)} %param.11) | data formatting | bytes 1835008 | tf_op args[4]
  2.3 0.0 copy-done
  2.3 1.3 %copy.9.up_hbm = bf16[1,1024,448]{2,1,0:T(8,128)(2,1)} copy(bf16[1,1024,448]{1,2,0:T(8,128)(2,1)S(1)} %copy-done) | data formatting | bytes 1835008 | tf_op args[5]
  3.7 49.8 %experts.1 = bf16[16,128]{1,0:T(8,128)(2,1)} custom-call(bf16[16,1024]{1,0:T(8,128)(2,1)} %tokens_hbm.1, f32[1,1024]{1,0:T(1,128)} %bitcast.3, s32[2,16]{1,0:T(2,128)} %bitcast.4, f32[2,16]{1,0:T(2,128)} %bitcast.5, bf16[1,1024,448]{2,1,0:T(8,128)(2,1)} %copy.8.gate_hbm, bf16[1,1024,448]{2,1,0:T(8,128)(2,1)} %copy.9.up_hbm, bf16[1,448,1024]{2,1,0:T(8,128)(2,1)} %down_hbm.1), custom_call_target="tpu_custom_call" | custom-call | tf_op jit(solution)/shard_map/experts/pallas_call | solution.py:156
  53.5 1.3 %copy.11 = bf16[16,128]{1,0:T(8,128)(2,1)} copy(bf16[16,128]{1,0:T(8,128)(2,1)} %experts.1) | data formatting | bytes 8192
Async XLA Ops:
  0.0 2.3 %copy-start = (bf16[1,1024,448]{1,2,0:T(8,128)(2,1)S(1)}, bf16[1,1024,448]{1,2,0:T(8,128)(2,1)}, u32[]{:S(2)}) copy-start(bf16[1,1024,448]{1,2,0:T(8,128)(2,1)} %param.12) | copy-start | bytes 2752516
where the time goes:
time: 54.9 us; the launch traced here: 54.7 us
  Pallas kernels  49.8 us (91%)
  local copies, waits for them, and re-layouts  4.92 us (9%)
    pallas_call x1, Pallas kernels, local(): pl.pallas_call(functools.partial(kernel, groups, shares), out_shape=jax.S...  49.8 us
    unnamed x5, local copies, waits for them, and re-layouts  4.92 us

commit v1 on v0

v1 whole, which is shorter than its diff:
```python
import functools

import jax
import jax.numpy as jnp
from jax import lax
from jax.experimental import pallas as pl
from jax.experimental.pallas import tpu as pltpu
from jax.sharding import PartitionSpec as P

CAP = 8
MESH = pl.DeviceIdType.MESH

norm_eps = 1e-06


def kernel(groups, shares, tokens_hbm, gain_hbm, routing_hbm, route_weight_hbm, gate_hbm, up_hbm, down_hbm, mixed,
           tokens, gain, routing, route_weight, gate, up, down,
           outgoing, incoming, partial, reduced, back, arrived,
           load_sem, swap_send, swap_recv, out_sem, in_sem, part_send, part_recv, back_send, back_recv):
    ep, tp = lax.axis_index("ep"), lax.axis_index("tp")
    width = tokens.shape[1]
    part = mixed.shape[1]
    half = groups // 2
    rows = half * CAP
    planes = shares // 2
    share = gate_hbm.shape[1]
    y, core = tp // 2, lax.rem(tp, 2)
    place, parity = ep // 2, lax.rem(ep, 2)
    own = (core == parity).astype(jnp.int32)
    shift = half // 4
    tile = 2 * part

    def group(q):
        return 2 * lax.rem(place + q, half) + core

    pairs = ((tokens_hbm, tokens), (gain_hbm, gain), (routing_hbm, routing), (route_weight_hbm, route_weight),
             (gate_hbm.at[0], gate.at[0:share]), (up_hbm.at[0], up.at[0:share]), (down_hbm.at[0], down.at[0:share]))
    loads = [pltpu.make_async_copy(source, target, load_sem.at[i]) for i, (source, target) in enumerate(pairs)]
    for i in (2, 3, 0, 1, 4, 5, 6):
        loads[i].start()

    far_first = sorted(range(half), key=lambda q: -min(q, half - q))
    barrier = pltpu.get_barrier_semaphore()
    for q in far_first:
        def greet(q=q):
            pl.semaphore_signal(barrier, inc=1, device_id=(group(q), 2 * y + parity), device_id_type=MESH)
        if q == 0:
            pl.when(core != parity)(greet)
        else:
            greet()
    for d in range(1, planes):
        pl.semaphore_signal(barrier, inc=1, device_id=(ep, 2 * lax.rem(y + d, planes) + core), device_id_type=MESH)
    pl.semaphore_signal(barrier, inc=1, device_id=(ep, 2 * y + 1 - core), device_id_type=MESH)

    count = tokens.shape[0]
    earlier = lax.broadcasted_iota(jnp.int32, (count, count), 0) < lax.broadcasted_iota(jnp.int32, (count, count), 1)
    earlier = jnp.where(earlier, 1.0, 0.0).astype(jnp.bfloat16)

    def slots_of(lines, expert_of):
        line = lax.broadcasted_iota(jnp.int32, (lines, count), 0)
        expert = expert_of(line // CAP)
        member = jnp.zeros((lines, count), jnp.float32)
        weight = jnp.zeros((lines, count), jnp.float32)
        for k in range(routing.shape[0]):
            named = routing[k:k + 1, :] == expert
            member = jnp.where(named, 1.0, member)
            weight = jnp.where(named, route_weight[k:k + 1, :], weight)
        before = jnp.dot(member.astype(jnp.bfloat16), earlier, preferred_element_type=jnp.float32)
        placed = jnp.where(before == lax.rem(line, CAP).astype(jnp.float32), member, 0.0)
        return placed, weight

    loads[2].wait()
    loads[3].wait()
    placed, _ = slots_of(rows, lambda q: group(q))
    loads[0].wait()
    loads[1].wait()
    values = tokens[...].astype(jnp.float32)
    scale = lax.rsqrt(jnp.mean(values * values, axis=-1, keepdims=True) + norm_eps)
    normed = (values * scale * gain[...]).astype(jnp.bfloat16)
    sent = jnp.dot(placed.astype(jnp.bfloat16), normed, preferred_element_type=jnp.float32)
    outgoing[...] = sent.reshape(half, CAP, width).astype(jnp.bfloat16)
    for i in (4, 5, 6):
        loads[i].wait()

    pl.semaphore_wait(barrier, half + planes - own)

    for q in far_first:
        at = (2 * half - q - shift) % half

        def dispatch(q=q, at=at):
            pltpu.make_async_remote_copy(
                src_ref=outgoing.at[q], dst_ref=incoming.at[at], send_sem=out_sem, recv_sem=in_sem,
                device_id=(group(q), 2 * y + parity), device_id_type=MESH).start()

        def keep(q=q, at=at):
            incoming[at] = outgoing[q]
        if q == 0:
            pl.when(core != parity)(dispatch)
            pl.when(core == parity)(keep)
        else:
            dispatch()

    swaps = [pltpu.make_async_remote_copy(
        src_ref=ref.at[0:share], dst_ref=ref.at[share:2 * share], send_sem=swap_send.at[i], recv_sem=swap_recv.at[i],
        device_id=(ep, 2 * y + 1 - core), device_id_type=MESH) for i, ref in enumerate((gate, up, down))]
    for swap in swaps:
        swap.start()

    picked, weight = slots_of(groups * CAP, lambda q: q)
    weight = jnp.transpose(weight * picked)

    for swap in swaps:
        swap.wait_recv()

    def wait_for(ref, sem, most):
        less, full = ref.at[pl.ds(0, most - 1)], ref.at[pl.ds(0, most)]
        pl.when(core == parity)(lambda: pltpu.make_async_copy(less, less, sem).wait())
        pl.when(core != parity)(lambda: pltpu.make_async_copy(full, full, sem).wait())
    wait_for(incoming, in_sem, half)

    x = incoming[...].astype(jnp.float32).reshape(rows, width).astype(jnp.bfloat16)
    last = (((1,), (1,)), ((), ()))
    gate_act = lax.dot_general(x, gate[...], last, preferred_element_type=jnp.float32)
    up_act = lax.dot_general(x, up[...], last, preferred_element_type=jnp.float32)
    hidden = (gate_act / (1.0 + jnp.exp(-gate_act)) * up_act).astype(jnp.bfloat16)

    chunks = 2
    piece = rows // chunks
    order = sorted(range(1, planes), key=lambda d: -min(d, planes - d))

    def columns(d):
        return pl.ds(pl.multiple_of(lax.rem(y + d, planes) * tile, tile), tile)

    def give(d, k):
        some = pl.ds(k * piece, piece)
        return pltpu.make_async_remote_copy(
            src_ref=partial.at[d - 1, some], dst_ref=reduced.at[d - 1, some],
            send_sem=part_send.at[d - 1, k], recv_sem=part_recv.at[d - 1, k],
            device_id=(ep, 2 * lax.rem(y + d, planes) + core), device_id_type=MESH)
    for d in order:
        partial[d - 1] = jnp.dot(hidden, down[:, columns(d)], preferred_element_type=jnp.float32)
        give(d, 0).start()
    for k in range(1, chunks):
        for d in order:
            give(d, k).start()
    total = jnp.dot(hidden, down[:, columns(0)], preferred_element_type=jnp.float32)

    def home(q):
        return lax.rem(q + shift, half)

    for k in range(chunks):
        mine = total[k * piece:(k + 1) * piece]
        for d in range(1, planes):
            give(d, k).wait_recv()
        for d in range(1, planes):
            mine = mine + reduced[d - 1, k * piece:(k + 1) * piece]
        first = k * (half // chunks)
        upto = first + half // chunks
        for side in range(2):
            back[side, first:upto] = mine[:, side * part:(side + 1) * part].reshape(half // chunks, CAP, part)
        distance = {at: min((at + shift) % half, half - (at + shift) % half) for at in range(first, upto)}
        for at in sorted(distance, key=lambda at: -distance[at]):
            for side in range(2):
                def send(at=at, side=side):
                    pltpu.make_async_remote_copy(
                        src_ref=back.at[side, at], dst_ref=arrived.at[ep], send_sem=back_send, recv_sem=back_recv,
                        device_id=(group(at + shift), 2 * y + side), device_id_type=MESH).start()

                def hold(at=at, side=side):
                    arrived[ep] = back[side, at]
                if distance[at] == 0:
                    here = jnp.logical_and(core == parity, core == side)
                    pl.when(here)(hold)
                    pl.when(jnp.logical_not(here))(send)
                else:
                    send()

    wait_for(arrived, back_recv, groups)
    out = jnp.dot(weight, arrived[...].reshape(groups * CAP, part), precision=lax.Precision.HIGHEST,
                  preferred_element_type=jnp.float32)
    mixed[...] = out.astype(mixed.dtype)
    wait_for(outgoing, out_sem, half)
    for swap in swaps:
        swap.wait_send()
    for k in range(chunks):
        for d in range(1, planes):
            give(d, k).wait_send()
    wait_for(arrived, back_send, groups)


def solution(mesh):
    groups, shares = mesh.shape["ep"], mesh.shape["tp"]

    def local(tokens, norm_gain, routing, route_weight, w_gate, w_up, w_down):
        count, width = tokens.shape
        part = width // shares
        half, planes = groups // 2, shares // 2
        rows = half * CAP
        share = w_down.shape[1]
        vmem = pl.BlockSpec(memory_space=pltpu.VMEM)
        hbm = pl.BlockSpec(memory_space=pltpu.HBM)
        return pl.pallas_call(
            functools.partial(kernel, groups, shares),
            out_shape=jax.ShapeDtypeStruct((count, part), jnp.bfloat16),
            in_specs=[hbm] * 7,
            out_specs=vmem,
            scratch_shapes=[
                pltpu.VMEM((count, width), tokens.dtype),
                pltpu.VMEM((1, width), norm_gain.dtype),
                pltpu.VMEM(routing.shape[::-1], routing.dtype),
                pltpu.VMEM(route_weight.shape[::-1], route_weight.dtype),
                pltpu.VMEM((2 * share, width), jnp.bfloat16),
                pltpu.VMEM((2 * share, width), jnp.bfloat16),
                pltpu.VMEM((2 * share, width), jnp.bfloat16),
                pltpu.VMEM((half, CAP, width), jnp.bfloat16),
                pltpu.VMEM((half, CAP, width), jnp.bfloat16),
                pltpu.VMEM((planes - 1, rows, 2 * part), jnp.float32),
                pltpu.VMEM((planes - 1, rows, 2 * part), jnp.float32),
                pltpu.VMEM((2, half, CAP, part), jnp.float32),
                pltpu.VMEM((groups, CAP, part), jnp.float32),
                pltpu.SemaphoreType.DMA((7,)),
                pltpu.SemaphoreType.DMA((3,)),
                pltpu.SemaphoreType.DMA((3,)),
                pltpu.SemaphoreType.DMA,
                pltpu.SemaphoreType.DMA,
                pltpu.SemaphoreType.DMA((planes - 1, 2)),
                pltpu.SemaphoreType.DMA((planes - 1, 2)),
                pltpu.SemaphoreType.DMA,
                pltpu.SemaphoreType.DMA,
            ],
            compiler_params=pltpu.CompilerParams(collective_id=0, has_side_effects=True,
                                                 vmem_limit_bytes=67043328),
            name="experts",
        )(tokens, norm_gain.reshape(1, width), routing.T, route_weight.T,
          jnp.swapaxes(w_gate, 1, 2), jnp.swapaxes(w_up, 1, 2), w_down)

    in_specs = (
        P("ep", None),
        P(),
        P("ep", None),
        P("ep", None),
        P("ep", None, "tp"),
        P("ep", None, "tp"),
        P("ep", "tp", None),
    )
    return jax.shard_map(local, mesh=mesh, in_specs=in_specs, out_specs=P("ep", "tp"), check_vma=False)
```

time: 54.9 us -> 38.3 us (0.70)
  Pallas kernels: 49.8 us -> 36.9 us
  local copies, waits for them, and re-layouts: 4.92 us -> 1.28 us
    pallas_call x1, Pallas kernels: 49.8 us -> 36.9 us  [local(): pl.pallas_call(functools.partial(kernel, groups, shares), out_shape=jax.S...]
    unnamed x5 -> x1, local copies, waits for them, and re-layouts: 4.92 us -> 1.28 us
where the time goes in v1:
time: 38.3 us; the launch traced here: 38.2 us
  Pallas kernels  36.9 us (96%)
  local copies, waits for them, and re-layouts  1.28 us (3%)
    pallas_call x1, Pallas kernels, local(): pl.pallas_call(functools.partial(kernel, groups, shares), out_shape=jax.S...  36.9 us
    unnamed x1, local copies, waits for them, and re-layouts  1.28 us

profile of v1, /device:TPU:1, one launch (start us, length us, event | category | flops | bytes accessed | tf_op | source)
XLA Modules:
  0.0 38.2 jit_solution(16470310219913419880)
XLA Ops:
  0.0 36.9 %experts.1 = bf16[16,128]{1,0:T(8,128)(2,1)} custom-call(bf16[16,1024]{1,0:T(8,128)(2,1)} %tokens_hbm.1, f32[1,1024]{1,0:T(1,128)} %bitcast.7, s32[2,16]{1,0:T(2,128)} %bitcast.8, f32[2,16]{1,0:T(2,128)} %bitcast.9, bf16[1,448,1024]{2,1,0:T(8,128)(2,1)} %bitcast.5, bf16[1,448,1024]{2,1,0:T(8,128)(2,1)} %bitcast.6, bf16[1,448,1024]{2,1,0:T(8,128)(2,1)} %down_hbm.1), custom_call_target="tpu_custom_call" | custom-call | tf_op jit(solution)/shard_map/experts/pallas_call | solution.py:202
  36.9 1.3 %copy.9 = bf16[16,128]{1,0:T(8,128)(2,1)} copy(bf16[16,128]{1,0:T(8,128)(2,1)} %experts.1) | data formatting | bytes 8192

commit v2 on v1

v2 whole, which is shorter than its diff:
```python
import functools

import jax
import jax.numpy as jnp
from jax import lax
from jax.experimental import pallas as pl
from jax.experimental.pallas import tpu as pltpu
from jax.sharding import PartitionSpec as P

CAP = 8
XS = 4
CHUNKS = ((0, 3), (3, 5), (5, 8))
MESH = pl.DeviceIdType.MESH

norm_eps = 1e-06


def kernel(groups, shares, tokens_hbm, gain_hbm, routing_hbm, route_weight_hbm, gate_hbm, up_hbm, down_hbm, mixed,
           tokens, gain, routing, route_weight, gate, up, down,
           row_tokens, row_routing, outgoing, incoming, partial, reduced, back, arrived,
           load_sem, row_send, row_recv, swap_send, swap_recv, out_sem, in_sem,
           part_send, part_recv, back_send, back_recv):
    ep, tp = lax.axis_index("ep"), lax.axis_index("tp")
    count, width = tokens.shape
    part = mixed.shape[1]
    zs = groups // XS
    planes = shares // 2
    share = gate_hbm.shape[1]
    tile = 2 * part
    z, x = ep // XS, lax.rem(ep, XS)
    y, core = tp // 2, lax.rem(tp, 2)
    parity = lax.rem(x, 2)
    same = core == parity

    offset = [(p + 1) // 2 if p % 2 else (zs - p // 2) % zs for p in range(zs)]
    position = {r: p for p, r in enumerate(offset)}

    def device(dz, to_x, dy, to_core):
        return (XS * lax.rem(z + dz, zs) + to_x, 2 * lax.rem(y + dy, planes) + to_core)

    def signal(target):
        pl.semaphore_signal(barrier, inc=1, device_id=target, device_id_type=MESH)

    def remote(src, dst, send, recv, target):
        return pltpu.make_async_remote_copy(src_ref=src, dst_ref=dst, send_sem=send, recv_sem=recv,
                                            device_id=target, device_id_type=MESH)

    far_first = sorted(range(1, zs), key=lambda q: -min(q, zs - q))
    barrier = pltpu.get_barrier_semaphore()
    for q in far_first:
        signal(device(q, x, 0, core))
    row_mate = [device(0, lax.rem(x + lax.rem(core + parity, 2) + 2 * v, XS), 0, parity) for v in range(2)]
    signal(row_mate[1])
    pl.when(jnp.logical_not(same))(lambda: signal(row_mate[0]))
    for d in (2, 1, 3):
        signal(device(0, x, d, core))
    partner = device(0, x, 0, 1 - core)
    signal(partner)

    pairs = ((tokens_hbm, tokens), (gain_hbm, gain), (routing_hbm, routing), (route_weight_hbm, route_weight),
             (gate_hbm.at[0], gate.at[0:share]), (up_hbm.at[0], up.at[0:share]), (down_hbm.at[0], down.at[0:share]))
    loads = [pltpu.make_async_copy(source, target, load_sem.at[i]) for i, (source, target) in enumerate(pairs)]
    for i in (0, 2, 1, 3, 4, 5, 6):
        loads[i].start()

    loads[0].wait()
    loads[2].wait()
    pl.semaphore_wait(barrier, zs - 1 + planes - 1 + 1 + 2 - same.astype(jnp.int32))

    def to_mate(v):
        remote(tokens, row_tokens.at[x // 2], row_send.at[0], row_recv.at[0], row_mate[v]).start()
        remote(routing, row_routing.at[x // 2], row_send.at[1], row_recv.at[1], row_mate[v]).start()
    to_mate(1)
    pl.when(jnp.logical_not(same))(lambda: to_mate(0))

    @pl.when(same)
    def _():
        row_tokens[x // 2] = tokens[...]
        row_routing[x // 2] = routing[...]

    loads[1].wait()
    loads[3].wait()
    for i in (4, 5, 6):
        loads[i].wait()
    swaps = [remote(ref.at[0:share], ref.at[share:2 * share], swap_send.at[i], swap_recv.at[i], partner)
             for i, ref in enumerate((gate, up, down))]
    for swap in swaps:
        swap.start()

    def wait_bytes(ref, number, sem):
        some = ref.at[pl.ds(0, number)]
        pltpu.make_async_copy(some, some, sem).wait()

    def wait_rows(sems):
        for ref, sem in zip((row_tokens, row_routing), sems):
            pl.when(same)(lambda ref=ref, sem=sem: wait_bytes(ref, 1, sem))
            pl.when(jnp.logical_not(same))(lambda ref=ref, sem=sem: wait_bytes(ref, 2, sem))
    wait_rows((row_recv.at[0], row_recv.at[1]))

    earlier = lax.broadcasted_iota(jnp.int32, (count, count), 0) < lax.broadcasted_iota(jnp.int32, (count, count), 1)
    earlier = jnp.where(earlier, 1.0, 0.0).astype(jnp.bfloat16)

    def slots_of(lines, expert_of, chosen, weights=None):
        line = lax.broadcasted_iota(jnp.int32, (lines, count), 0)
        expert = expert_of(line // CAP)
        member = jnp.zeros((lines, count), jnp.float32)
        weight = jnp.zeros((lines, count), jnp.float32)
        for k in range(chosen.shape[0]):
            named = chosen[k:k + 1, :] == expert
            member = jnp.where(named, 1.0, member)
            if weights is not None:
                weight = jnp.where(named, weights[k:k + 1, :], weight)
        before = jnp.dot(member.astype(jnp.bfloat16), earlier, preferred_element_type=jnp.float32)
        placed = jnp.where(before == lax.rem(line, CAP).astype(jnp.float32), member, 0.0)
        return placed, weight

    for u in range(2):
        placed, _ = slots_of(zs * CAP, lambda q: XS * lax.rem(z + q, zs) + x, row_routing[u])
        values = row_tokens[u].astype(jnp.float32)
        scale = lax.rsqrt(jnp.mean(values * values, axis=-1, keepdims=True) + norm_eps)
        normed = (values * scale * gain[...]).astype(jnp.bfloat16)
        sent = jnp.dot(placed.astype(jnp.bfloat16), normed, preferred_element_type=jnp.float32)
        outgoing[:, u] = sent.reshape(zs, CAP, width).astype(jnp.bfloat16)

    chunk_of = {p: k for k, (first, upto) in enumerate(CHUNKS) for p in range(first, upto)}
    for q in far_first:
        p = position[(zs - q) % zs]
        remote(outgoing.at[q], incoming.at[p], out_sem, in_sem.at[chunk_of[p]], device(q, x, 0, core)).start()
    incoming[0] = outgoing[0]

    def expert_at(place):
        p = place // XS
        away = jnp.where(lax.rem(p, 2) == 1, (p + 1) // 2, zs - p // 2)
        return XS * lax.rem(z - away + zs, zs) + lax.rem(place, XS)
    picked, weight = slots_of(groups * CAP, expert_at, routing[...], route_weight[...])
    weight = jnp.transpose(weight * picked)

    for swap in swaps:
        swap.wait_recv()

    def columns(d):
        return pl.ds(pl.multiple_of(lax.rem(y + d, planes) * tile, tile), tile)

    def give(d, k):
        first, upto = CHUNKS[k]
        some = pl.ds(first * 2 * CAP, (upto - first) * 2 * CAP)
        return remote(partial.at[d - 1, some], reduced.at[d - 1, some], part_send.at[d - 1, k], part_recv.at[d - 1, k],
                      device(0, x, d, core))

    last = (((1,), (1,)), ((), ()))
    totals = []
    for k, (first, upto) in enumerate(CHUNKS):
        wait_bytes(incoming, upto - max(first, 1), in_sem.at[k])
        rows = (upto - first) * 2 * CAP
        here = slice(first * 2 * CAP, upto * 2 * CAP)
        a = incoming[first:upto].astype(jnp.float32).reshape(rows, width).astype(jnp.bfloat16)
        gate_act = lax.dot_general(a, gate[...], last, preferred_element_type=jnp.float32)
        up_act = lax.dot_general(a, up[...], last, preferred_element_type=jnp.float32)
        hidden = (gate_act / (1.0 + jnp.exp(-gate_act)) * up_act).astype(jnp.bfloat16)
        for d in (2, 1, 3):
            partial[d - 1, here] = jnp.dot(hidden, down[:, columns(d)], preferred_element_type=jnp.float32)
            give(d, k).start()
        totals.append(jnp.dot(hidden, down[:, columns(0)], preferred_element_type=jnp.float32))

    for k, (first, upto) in enumerate(CHUNKS):
        here = slice(first * 2 * CAP, upto * 2 * CAP)
        mine = totals[k]
        for d in (1, 3, 2):
            give(d, k).wait_recv()
            mine = mine + reduced[d - 1, here]
        for side in range(2):
            back[side, first:upto] = mine[:, side * part:(side + 1) * part].reshape(upto - first, 2, CAP, part)
        for p in reversed(range(first, upto)):
            for u in range(2):
                to_x = core + 2 * u
                for side in range(2):
                    def send(p=p, u=u, side=side, to_x=to_x, k=k):
                        remote(back.at[side, p, u], arrived.at[p * XS + x], back_send, back_recv.at[k],
                               device(offset[p], to_x, 0, side)).start()

                    def hold(p=p, u=u, side=side):
                        arrived[p * XS + x] = back[side, p, u]
                    if p == 0:
                        mine_too = jnp.logical_and(to_x == x, core == side)
                        pl.when(mine_too)(hold)
                        pl.when(jnp.logical_not(mine_too))(send)
                    else:
                        send()

    def wait_blocks(number, own_too, sem):
        if own_too:
            pl.when(same)(lambda: wait_bytes(arrived, number - 1, sem))
            pl.when(jnp.logical_not(same))(lambda: wait_bytes(arrived, number, sem))
        else:
            wait_bytes(arrived, number, sem)

    flat = XS * CAP
    out = jnp.zeros((count, part), jnp.float32)
    for k, (first, upto) in enumerate(CHUNKS):
        wait_blocks((upto - first) * XS, first == 0, back_recv.at[k])
        out = out + jnp.dot(weight[:, first * flat:upto * flat], arrived[first * XS:upto * XS].reshape((upto - first) * flat, part),
                            precision=lax.Precision.HIGHEST, preferred_element_type=jnp.float32)
    mixed[...] = out.astype(mixed.dtype)

    wait_rows((row_send.at[0], row_send.at[1]))
    wait_bytes(outgoing, zs - 1, out_sem)
    for swap in swaps:
        swap.wait_send()
    for k in range(len(CHUNKS)):
        for d in range(1, planes):
            give(d, k).wait_send()
    wait_blocks(groups, True, back_send)


def solution(mesh):
    groups, shares = mesh.shape["ep"], mesh.shape["tp"]

    def local(tokens, norm_gain, routing, route_weight, w_gate, w_up, w_down):
        count, width = tokens.shape
        part = width // shares
        zs, planes = groups // XS, shares // 2
        rows = zs * 2 * CAP
        share = w_down.shape[1]
        chunks = len(CHUNKS)
        vmem = pl.BlockSpec(memory_space=pltpu.VMEM)
        hbm = pl.BlockSpec(memory_space=pltpu.HBM)
        dma = pltpu.SemaphoreType.DMA
        return pl.pallas_call(
            functools.partial(kernel, groups, shares),
            out_shape=jax.ShapeDtypeStruct((count, part), jnp.bfloat16),
            in_specs=[hbm] * 7,
            out_specs=vmem,
            scratch_shapes=[
                pltpu.VMEM((count, width), tokens.dtype),
                pltpu.VMEM((1, width), norm_gain.dtype),
                pltpu.VMEM(routing.shape[::-1], routing.dtype),
                pltpu.VMEM(route_weight.shape[::-1], route_weight.dtype),
                pltpu.VMEM((2 * share, width), jnp.bfloat16),
                pltpu.VMEM((2 * share, width), jnp.bfloat16),
                pltpu.VMEM((2 * share, width), jnp.bfloat16),
                pltpu.VMEM((2, count, width), tokens.dtype),
                pltpu.VMEM((2, *routing.shape[::-1]), routing.dtype),
                pltpu.VMEM((zs, 2, CAP, width), jnp.bfloat16),
                pltpu.VMEM((zs, 2, CAP, width), jnp.bfloat16),
                pltpu.VMEM((planes - 1, rows, 2 * part), jnp.float32),
                pltpu.VMEM((planes - 1, rows, 2 * part), jnp.float32),
                pltpu.VMEM((2, zs, 2, CAP, part), jnp.float32),
                pltpu.VMEM((groups, CAP, part), jnp.float32),
                dma((7,)), dma((2,)), dma((2,)), dma((3,)), dma((3,)), dma, dma((chunks,)),
                dma((planes - 1, chunks)), dma((planes - 1, chunks)), dma, dma((chunks,)),
            ],
            compiler_params=pltpu.CompilerParams(collective_id=0, has_side_effects=True,
                                                 vmem_limit_bytes=67043328),
            name="experts",
        )(tokens, norm_gain.reshape(1, width), routing.T, route_weight.T,
          jnp.swapaxes(w_gate, 1, 2), jnp.swapaxes(w_up, 1, 2), w_down)

    in_specs = (
        P("ep", None),
        P(),
        P("ep", None),
        P("ep", None),
        P("ep", None, "tp"),
        P("ep", None, "tp"),
        P("ep", "tp", None),
    )
    return jax.shard_map(local, mesh=mesh, in_specs=in_specs, out_specs=P("ep", "tp"), check_vma=False)
```

time: 38.3 us -> 42 us (1.097)
  Pallas kernels: 36.9 us -> 40.6 us
    pallas_call x1, Pallas kernels: 36.9 us -> 40.6 us  [local(): pl.pallas_call(functools.partial(kernel, groups, shares), out_shape=jax.S...]
where the time goes in v2:
time: 42 us; the launch traced here: 41.9 us
  Pallas kernels  40.6 us (97%)
  local copies, waits for them, and re-layouts  1.28 us (3%)
    pallas_call x1, Pallas kernels, local(): pl.pallas_call(functools.partial(kernel, groups, shares), out_shape=jax.S...  40.6 us
    unnamed x1, local copies, waits for them, and re-layouts  1.28 us

profile of v2, /device:TPU:1, one launch (start us, length us, event | category | flops | bytes accessed | tf_op | source)
XLA Modules:
  0.0 41.9 jit_solution(11234020277182750647)
XLA Ops:
  0.0 40.6 %experts.1 = bf16[16,128]{1,0:T(8,128)(2,1)} custom-call(bf16[16,1024]{1,0:T(8,128)(2,1)} %tokens_hbm.1, f32[1,1024]{1,0:T(1,128)} %bitcast.7, s32[2,16]{1,0:T(2,128)} %bitcast.8, f32[2,16]{1,0:T(2,128)} %bitcast.9, bf16[1,448,1024]{2,1,0:T(8,128)(2,1)} %bitcast.5, bf16[1,448,1024]{2,1,0:T(8,128)(2,1)} %bitcast.6, bf16[1,448,1024]{2,1,0:T(8,128)(2,1)} %down_hbm.1), custom_call_target="tpu_custom_call" | custom-call | tf_op jit(solution)/shard_map/experts/pallas_call | solution.py:228
  40.6 1.3 %copy.9 = bf16[16,128]{1,0:T(8,128)(2,1)} copy(bf16[16,128]{1,0:T(8,128)(2,1)} %experts.1) | data formatting | bytes 8192

commit v3 on v1

--- a/solution.py
+++ b/solution.py
@@ -8,13 +8,16 @@
 from jax.sharding import PartitionSpec as P
 
 CAP = 8
+CHUNKS = ((0, 16),)
+PIECES = (((12, 16), (8, 12), (4, 8), (0, 4)),)
+STEPS = ('c0', 'r0', 'r1', 'r2', 'r3')
 MESH = pl.DeviceIdType.MESH
 
 norm_eps = 1e-06
 
 
 def kernel(groups, shares, tokens_hbm, gain_hbm, routing_hbm, route_weight_hbm, gate_hbm, up_hbm, down_hbm, mixed,
-           tokens, gain, routing, route_weight, gate, up, down,
+           tokens, gain, routing, route_weight, gate, up, down, gate_across, up_across,
            outgoing, incoming, partial, reduced, back, arrived,
            load_sem, swap_send, swap_recv, out_sem, in_sem, part_send, part_recv, back_send, back_recv):
     ep, tp = lax.axis_index("ep"), lax.axis_index("tp")
@@ -27,7 +30,9 @@
     y, core = tp // 2, lax.rem(tp, 2)
     place, parity = ep // 2, lax.rem(ep, 2)
     own = (core == parity).astype(jnp.int32)
-    shift = half // 4
+    offset = sorted(range(half), key=lambda q: min(q, half - q))
+    position = {q: p for p, q in enumerate(offset)}
+    chunk_of = {p: k for k, (first, upto) in enumerate(CHUNKS) for p in range(first, upto)}
     tile = 2 * part
 
     def group(q):
@@ -79,17 +84,15 @@
     normed = (values * scale * gain[...]).astype(jnp.bfloat16)
     sent = jnp.dot(placed.astype(jnp.bfloat16), normed, preferred_element_type=jnp.float32)
     outgoing[...] = sent.reshape(half, CAP, width).astype(jnp.bfloat16)
-    for i in (4, 5, 6):
-        loads[i].wait()
 
     pl.semaphore_wait(barrier, half + planes - own)
 
     for q in far_first:
-        at = (2 * half - q - shift) % half
+        at = position[(half - q) % half]
 
         def dispatch(q=q, at=at):
             pltpu.make_async_remote_copy(
-                src_ref=outgoing.at[q], dst_ref=incoming.at[at], send_sem=out_sem, recv_sem=in_sem,
+                src_ref=outgoing.at[q], dst_ref=incoming.at[at], send_sem=out_sem, recv_sem=in_sem.at[chunk_of[at]],
                 device_id=(group(q), 2 * y + parity), device_id_type=MESH).start()
 
         def keep(q=q, at=at):
@@ -103,6 +106,8 @@
     swaps = [pltpu.make_async_remote_copy(
         src_ref=ref.at[0:share], dst_ref=ref.at[share:2 * share], send_sem=swap_send.at[i], recv_sem=swap_recv.at[i],
         device_id=(ep, 2 * y + 1 - core), device_id_type=MESH) for i, ref in enumerate((gate, up, down))]
+    for i in (4, 5, 6):
+        loads[i].wait()
     for swap in swaps:
         swap.start()
 
@@ -111,69 +116,78 @@
 
     for swap in swaps:
         swap.wait_recv()
+    gate_across[...] = jnp.transpose(gate[...])
+    up_across[...] = jnp.transpose(up[...])
 
     def wait_for(ref, sem, most):
         less, full = ref.at[pl.ds(0, most - 1)], ref.at[pl.ds(0, most)]
         pl.when(core == parity)(lambda: pltpu.make_async_copy(less, less, sem).wait())
         pl.when(core != parity)(lambda: pltpu.make_async_copy(full, full, sem).wait())
-    wait_for(incoming, in_sem, half)
-
-    x = incoming[...].astype(jnp.float32).reshape(rows, width).astype(jnp.bfloat16)
-    last = (((1,), (1,)), ((), ()))
-    gate_act = lax.dot_general(x, gate[...], last, preferred_element_type=jnp.float32)
-    up_act = lax.dot_general(x, up[...], last, preferred_element_type=jnp.float32)
-    hidden = (gate_act / (1.0 + jnp.exp(-gate_act)) * up_act).astype(jnp.bfloat16)
-
-    chunks = 2
-    piece = rows // chunks
+
     order = sorted(range(1, planes), key=lambda d: -min(d, planes - d))
+    pieces = [piece for some in PIECES for piece in some]
+    totals = {}
 
     def columns(d):
         return pl.ds(pl.multiple_of(lax.rem(y + d, planes) * tile, tile), tile)
 
-    def give(d, k):
-        some = pl.ds(k * piece, piece)
+    def give(d, piece):
+        some = pl.ds(piece[0] * CAP, (piece[1] - piece[0]) * CAP)
+        sems = part_send.at[d - 1, pieces.index(piece)], part_recv.at[d - 1, pieces.index(piece)]
         return pltpu.make_async_remote_copy(
-            src_ref=partial.at[d - 1, some], dst_ref=reduced.at[d - 1, some],
-            send_sem=part_send.at[d - 1, k], recv_sem=part_recv.at[d - 1, k],
+            src_ref=partial.at[d - 1, some], dst_ref=reduced.at[d - 1, some], send_sem=sems[0], recv_sem=sems[1],
             device_id=(ep, 2 * lax.rem(y + d, planes) + core), device_id_type=MESH)
-    for d in order:
-        partial[d - 1] = jnp.dot(hidden, down[:, columns(d)], preferred_element_type=jnp.float32)
-        give(d, 0).start()
-    for k in range(1, chunks):
+
+    def multiply(k):
+        first, upto = CHUNKS[k]
+        if first == 0:
+            wait_for(incoming, in_sem.at[k], upto)
+        else:
+            some = incoming.at[pl.ds(first, upto - first)]
+            pltpu.make_async_copy(some, some, in_sem.at[k]).wait()
+        x = incoming[first:upto].astype(jnp.float32).reshape((upto - first) * CAP, width).astype(jnp.bfloat16)
+        gate_act = jnp.dot(x, gate_across[...], preferred_element_type=jnp.float32)
+        up_act = jnp.dot(x, up_across[...], preferred_element_type=jnp.float32)
+        hidden = (gate_act / (1.0 + jnp.exp(-gate_act)) * up_act).astype(jnp.bfloat16)
         for d in order:
-            give(d, k).start()
-    total = jnp.dot(hidden, down[:, columns(0)], preferred_element_type=jnp.float32)
-
-    def home(q):
-        return lax.rem(q + shift, half)
-
-    for k in range(chunks):
-        mine = total[k * piece:(k + 1) * piece]
+            partial[d - 1, first * CAP:upto * CAP] = jnp.dot(hidden, down[:, columns(d)],
+                                                             preferred_element_type=jnp.float32)
+            give(d, PIECES[k][0]).start()
+        for piece in PIECES[k][1:]:
+            for d in order:
+                give(d, piece).start()
+        mine = jnp.dot(hidden, down[:, columns(0)], preferred_element_type=jnp.float32)
+        for piece in PIECES[k]:
+            totals[piece] = mine[(piece[0] - first) * CAP:(piece[1] - first) * CAP]
+
+    def give_back(k):
+        piece = pieces[k]
+        first, upto = piece
+        mine = totals[piece]
         for d in range(1, planes):
-            give(d, k).wait_recv()
+            give(d, piece).wait_recv()
         for d in range(1, planes):
-            mine = mine + reduced[d - 1, k * piece:(k + 1) * piece]
-        first = k * (half // chunks)
-        upto = first + half // chunks
+            mine = mine + reduced[d - 1, first * CAP:upto * CAP]
         for side in range(2):
-            back[side, first:upto] = mine[:, side * part:(side + 1) * part].reshape(half // chunks, CAP, part)
-        distance = {at: min((at + shift) % half, half - (at + shift) % half) for at in range(first, upto)}
-        for at in sorted(distance, key=lambda at: -distance[at]):
+            back[side, first:upto] = mine[:, side * part:(side + 1) * part].reshape(upto - first, CAP, part)
+        for at in reversed(range(first, upto)):
             for side in range(2):
                 def send(at=at, side=side):
                     pltpu.make_async_remote_copy(
                         src_ref=back.at[side, at], dst_ref=arrived.at[ep], send_sem=back_send, recv_sem=back_recv,
-                        device_id=(group(at + shift), 2 * y + side), device_id_type=MESH).start()
+                        device_id=(group(offset[at]), 2 * y + side), device_id_type=MESH).start()
 
                 def hold(at=at, side=side):
                     arrived[ep] = back[side, at]
-                if distance[at] == 0:
+                if at == 0:
                     here = jnp.logical_and(core == parity, core == side)
                     pl.when(here)(hold)
                     pl.when(jnp.logical_not(here))(send)
                 else:
                     send()
+
+    for step in STEPS:
+        (multiply if step[0] == "c" else give_back)(int(step[1:]))
 
     wait_for(arrived, back_recv, groups)
     out = jnp.dot(weight, arrived[...].reshape(groups * CAP, part), precision=lax.Precision.HIGHEST,
@@ -182,9 +196,9 @@
     wait_for(outgoing, out_sem, half)
     for swap in swaps:
         swap.wait_send()
-    for k in range(chunks):
+    for piece in pieces:
         for d in range(1, planes):
-            give(d, k).wait_send()
+            give(d, piece).wait_send()
     wait_for(arrived, back_send, groups)
 
 
@@ -197,11 +211,12 @@
         half, planes = groups // 2, shares // 2
         rows = half * CAP
         share = w_down.shape[1]
+        pieces = sum(map(len, PIECES))
         vmem = pl.BlockSpec(memory_space=pltpu.VMEM)
         hbm = pl.BlockSpec(memory_space=pltpu.HBM)
         return pl.pallas_call(
             functools.partial(kernel, groups, shares),
-            out_shape=jax.ShapeDtypeStruct((count, part), jnp.bfloat16),
+            out_shape=pltpu.VMEM((count, part), jnp.bfloat16),
             in_specs=[hbm] * 7,
             out_specs=vmem,
             scratch_shapes=[
@@ -212,6 +227,8 @@
                 pltpu.VMEM((2 * share, width), jnp.bfloat16),
                 pltpu.VMEM((2 * share, width), jnp.bfloat16),
                 pltpu.VMEM((2 * share, width), jnp.bfloat16),
+                pltpu.VMEM((width, 2 * share), jnp.bfloat16),
+                pltpu.VMEM((width, 2 * share), jnp.bfloat16),
                 pltpu.VMEM((half, CAP, width), jnp.bfloat16),
                 pltpu.VMEM((half, CAP, width), jnp.bfloat16),
                 pltpu.VMEM((planes - 1, rows, 2 * part), jnp.float32),
@@ -222,14 +239,14 @@
                 pltpu.SemaphoreType.DMA((3,)),
                 pltpu.SemaphoreType.DMA((3,)),
                 pltpu.SemaphoreType.DMA,
-                pltpu.SemaphoreType.DMA,
-                pltpu.SemaphoreType.DMA((planes - 1, 2)),
-                pltpu.SemaphoreType.DMA((planes - 1, 2)),
+                pltpu.SemaphoreType.DMA((len(CHUNKS),)),
+                pltpu.SemaphoreType.DMA((planes - 1, pieces)),
+                pltpu.SemaphoreType.DMA((planes - 1, pieces)),
                 pltpu.SemaphoreType.DMA,
                 pltpu.SemaphoreType.DMA,
             ],
             compiler_params=pltpu.CompilerParams(collective_id=0, has_side_effects=True,
-                                                 vmem_limit_bytes=67043328),
+                                                 vmem_limit_bytes=67043328 - 16384),
             name="experts",
         )(tokens, norm_gain.reshape(1, width), routing.T, route_weight.T,
           jnp.swapaxes(w_gate, 1, 2), jnp.swapaxes(w_up, 1, 2), w_down)

time: 38.3 us -> 35.5 us (0.927)
  Pallas kernels: 36.9 us -> 34.8 us
  local copies, waits for them, and re-layouts: 1.28 us -> 0.6 us
    pallas_call x1, Pallas kernels: 36.9 us -> 34.8 us  [local(): pl.pallas_call(functools.partial(kernel, groups, shares), out_shape=pltpu...]
    unnamed x1, local copies, waits for them, and re-layouts: 1.28 us -> 0.6 us
where the time goes in v3:
time: 35.5 us; the launch traced here: 35.4 us
  Pallas kernels  34.8 us (98%)
  local copies, waits for them, and re-layouts  0.6 us (2%)
    pallas_call x1, Pallas kernels, local(): pl.pallas_call(functools.partial(kernel, groups, shares), out_shape=pltpu...  34.8 us

profile of v3, /device:TPU:1, one launch (start us, length us, event | category | flops | bytes accessed | tf_op | source)
XLA Modules:
  0.0 35.4 jit_solution(7499127028867359292)
XLA Ops:
  0.0 34.8 %experts.1 = bf16[16,128]{1,0:T(8,128)(2,1)S(1)} custom-call(bf16[16,1024]{1,0:T(8,128)(2,1)} %tokens_hbm.1, f32[1,1024]{1,0:T(1,128)} %bitcast.7, s32[2,16]{1,0:T(2,128)} %bitcast.8, f32[2,16]{1,0:T(2,128)} %bitcast.9, bf16[1,448,1024]{2,1,0:T(8,128)(2,1)} %bitcast.5, bf16[1,448,1024]{2,1,0:T(8,128)(2,1)} %bitcast.6, bf16[1,448,1024]{2,1,0:T(8,128)(2,1)} %down_hbm.1), custom_call_target="tpu_custom_call" | custom-call | tf_op jit(solution)/shard_map/experts/pallas_call | solution.py:217
  34.8 0.6 %copy.9 = bf16[16,128]{1,0:T(8,128)(2,1)} copy(bf16[16,128]{1,0:T(8,128)(2,1)S(1)} %experts.1) | data formatting | bytes 8192

commit v4 on v3

--- a/solution.py
+++ b/solution.py
@@ -11,6 +11,8 @@
 CHUNKS = ((0, 16),)
 PIECES = (((12, 16), (8, 12), (4, 8), (0, 4)),)
 STEPS = ('c0', 'r0', 'r1', 'r2', 'r3')
+STEPS_16 = 32767.0
+LEAST = 2e-34
 MESH = pl.DeviceIdType.MESH
 
 norm_eps = 1e-06
@@ -18,8 +20,8 @@
 
 def kernel(groups, shares, tokens_hbm, gain_hbm, routing_hbm, route_weight_hbm, gate_hbm, up_hbm, down_hbm, mixed,
            tokens, gain, routing, route_weight, gate, up, down, gate_across, up_across,
-           outgoing, incoming, partial, reduced, back, arrived,
-           load_sem, swap_send, swap_recv, out_sem, in_sem, part_send, part_recv, back_send, back_recv):
+           outgoing, incoming, partial, reduced, peak, their_peak, back, arrived,
+           load_sem, swap_send, swap_recv, out_sem, in_sem, part_send, part_recv, peak_send, peak_recv, back_send, back_recv):
     ep, tp = lax.axis_index("ep"), lax.axis_index("tp")
     width = tokens.shape[1]
     part = mixed.shape[1]
@@ -138,6 +140,11 @@
             src_ref=partial.at[d - 1, some], dst_ref=reduced.at[d - 1, some], send_sem=sems[0], recv_sem=sems[1],
             device_id=(ep, 2 * lax.rem(y + d, planes) + core), device_id_type=MESH)
 
+    def give_peak(d):
+        return pltpu.make_async_remote_copy(
+            src_ref=peak.at[d - 1], dst_ref=their_peak.at[d - 1], send_sem=peak_send.at[d - 1],
+            recv_sem=peak_recv.at[d - 1], device_id=(ep, 2 * lax.rem(y + d, planes) + core), device_id_type=MESH)
+
     def multiply(k):
         first, upto = CHUNKS[k]
         if first == 0:
@@ -150,8 +157,15 @@
         up_act = jnp.dot(x, up_across[...], preferred_element_type=jnp.float32)
         hidden = (gate_act / (1.0 + jnp.exp(-gate_act)) * up_act).astype(jnp.bfloat16)
         for d in order:
-            partial[d - 1, first * CAP:upto * CAP] = jnp.dot(hidden, down[:, columns(d)],
-                                                             preferred_element_type=jnp.float32)
+            block = jnp.dot(hidden, down[:, columns(d)], preferred_element_type=jnp.float32)
+            sides = [block[:, side * part:(side + 1) * part].reshape(upto - first, CAP, part) for side in range(2)]
+            most = jnp.maximum(jnp.max(jnp.maximum(jnp.abs(sides[0]), jnp.abs(sides[1])), axis=0), LEAST)
+            peak[d - 1] = most
+            give_peak(d).start()
+            for side in range(2):
+                coded = jnp.round(sides[side] * (STEPS_16 / most)).reshape((upto - first) * CAP, part)
+                partial[d - 1, first * CAP:upto * CAP, side * part:(side + 1) * part] = (
+                    coded.astype(jnp.int32).astype(jnp.int16))
             give(d, PIECES[k][0]).start()
         for piece in PIECES[k][1:]:
             for d in order:
@@ -165,11 +179,16 @@
         first, upto = piece
         mine = totals[piece]
         for d in range(1, planes):
+            if k == 0:
+                give_peak(d).wait_recv()
             give(d, piece).wait_recv()
-        for d in range(1, planes):
-            mine = mine + reduced[d - 1, first * CAP:upto * CAP]
         for side in range(2):
-            back[side, first:upto] = mine[:, side * part:(side + 1) * part].reshape(upto - first, CAP, part)
+            columns_here = slice(side * part, (side + 1) * part)
+            total = mine[:, columns_here].reshape(upto - first, CAP, part)
+            for d in range(1, planes):
+                coded = reduced[d - 1, first * CAP:upto * CAP, columns_here].astype(jnp.int32).astype(jnp.float32)
+                total = total + coded.reshape(upto - first, CAP, part) * (their_peak[d - 1] * (1.0 / STEPS_16))
+            back[side, first:upto] = total
         for at in reversed(range(first, upto)):
             for side in range(2):
                 def send(at=at, side=side):
@@ -196,6 +215,8 @@
     wait_for(outgoing, out_sem, half)
     for swap in swaps:
         swap.wait_send()
+    for d in range(1, planes):
+        give_peak(d).wait_send()
     for piece in pieces:
         for d in range(1, planes):
             give(d, piece).wait_send()
@@ -231,8 +252,10 @@
                 pltpu.VMEM((width, 2 * share), jnp.bfloat16),
                 pltpu.VMEM((half, CAP, width), jnp.bfloat16),
                 pltpu.VMEM((half, CAP, width), jnp.bfloat16),
-                pltpu.VMEM((planes - 1, rows, 2 * part), jnp.float32),
-                pltpu.VMEM((planes - 1, rows, 2 * part), jnp.float32),
+                pltpu.VMEM((planes - 1, rows, 2 * part), jnp.int16),
+                pltpu.VMEM((planes - 1, rows, 2 * part), jnp.int16),
+                pltpu.VMEM((planes - 1, CAP, part), jnp.float32),
+                pltpu.VMEM((planes - 1, CAP, part), jnp.float32),
                 pltpu.VMEM((2, half, CAP, part), jnp.float32),
                 pltpu.VMEM((groups, CAP, part), jnp.float32),
                 pltpu.SemaphoreType.DMA((7,)),
@@ -242,6 +265,8 @@
                 pltpu.SemaphoreType.DMA((len(CHUNKS),)),
                 pltpu.SemaphoreType.DMA((planes - 1, pieces)),
                 pltpu.SemaphoreType.DMA((planes - 1, pieces)),
+                pltpu.SemaphoreType.DMA((planes - 1,)),
+                pltpu.SemaphoreType.DMA((planes - 1,)),
                 pltpu.SemaphoreType.DMA,
                 pltpu.SemaphoreType.DMA,
             ],

time: 35.5 us -> 33.5 us (0.944)
  Pallas kernels: 34.8 us -> 32.8 us
    pallas_call x1, Pallas kernels: 34.8 us -> 32.8 us  [local(): pl.pallas_call(functools.partial(kernel, groups, shares), out_shape=pltpu...]
where the time goes in v4:
time: 33.5 us; the launch traced here: 33.4 us
  Pallas kernels  32.8 us (98%)
  local copies, waits for them, and re-layouts  0.6 us (2%)
    pallas_call x1, Pallas kernels, local(): pl.pallas_call(functools.partial(kernel, groups, shares), out_shape=pltpu...  32.8 us

profile of v4, /device:TPU:1, one launch (start us, length us, event | category | flops | bytes accessed | tf_op | source)
XLA Modules:
  0.0 33.4 jit_solution(4830514623649638416)
XLA Ops:
  0.0 32.8 %experts.1 = bf16[16,128]{1,0:T(8,128)(2,1)S(1)} custom-call(bf16[16,1024]{1,0:T(8,128)(2,1)} %tokens_hbm.1, f32[1,1024]{1,0:T(1,128)} %bitcast.7, s32[2,16]{1,0:T(2,128)} %bitcast.8, f32[2,16]{1,0:T(2,128)} %bitcast.9, bf16[1,448,1024]{2,1,0:T(8,128)(2,1)} %bitcast.5, bf16[1,448,1024]{2,1,0:T(8,128)(2,1)} %bitcast.6, bf16[1,448,1024]{2,1,0:T(8,128)(2,1)} %down_hbm.1), custom_call_target="tpu_custom_call" | custom-call | tf_op jit(solution)/shard_map/experts/pallas_call | solution.py:238
  32.8 0.6 %copy.9 = bf16[16,128]{1,0:T(8,128)(2,1)} copy(bf16[16,128]{1,0:T(8,128)(2,1)S(1)} %experts.1) | data formatting | bytes 8192

commit v5 on v4

--- a/solution.py
+++ b/solution.py
@@ -8,6 +8,7 @@
 from jax.sharding import PartitionSpec as P
 
 CAP = 8
+XS = 4
 CHUNKS = ((0, 16),)
 PIECES = (((12, 16), (8, 12), (4, 8), (0, 4)),)
 STEPS = ('c0', 'r0', 'r1', 'r2', 'r3')
@@ -16,6 +17,21 @@
 MESH = pl.DeviceIdType.MESH
 
 norm_eps = 1e-06
+
+
+def tables(zs, xs):
+    steps = [(dz, dx) for dz in range(zs) for dx in range(xs)]
+    inverse = {(dz, dx): ((zs - dz) % zs, (xs - dx) % xs) for dz, dx in steps}
+    hops = lambda step: min(step[0], zs - step[0]) + min(step[1], xs - step[1])
+    alone = sorted((step for step in steps if inverse[step] == step), key=hops)
+    paired = sorted((step for step in steps if step < inverse[step]), key=hops)
+    near, far = [], []
+    for some, single, double in ((near, alone[:2], paired[:len(paired) // 2]), (far, alone[2:], paired[len(paired) // 2:])):
+        some.append(single[0])
+        for step in double:
+            some += [step, inverse[step]]
+        some.append(single[1])
+    return near, far, [near.index(inverse[step]) for step in near]
 
 
 def kernel(groups, shares, tokens_hbm, gain_hbm, routing_hbm, route_weight_hbm, gate_hbm, up_hbm, down_hbm, mixed,
@@ -30,34 +46,32 @@
     planes = shares // 2
     share = gate_hbm.shape[1]
     y, core = tp // 2, lax.rem(tp, 2)
-    place, parity = ep // 2, lax.rem(ep, 2)
-    own = (core == parity).astype(jnp.int32)
-    offset = sorted(range(half), key=lambda q: min(q, half - q))
-    position = {q: p for p, q in enumerate(offset)}
+    near, far, back_at = tables(groups // XS, XS)
+
+    def group(p):
+        dz, dx = (n + (f - n) * core for n, f in zip(near[p], far[p]))
+        return XS * lax.rem(ep // XS + dz, groups // XS) + lax.rem(lax.rem(ep, XS) + dx, XS)
+
     chunk_of = {p: k for k, (first, upto) in enumerate(CHUNKS) for p in range(first, upto)}
     tile = 2 * part
 
-    def group(q):
-        return 2 * lax.rem(place + q, half) + core
+    barrier = pltpu.get_barrier_semaphore()
+    for p in reversed(range(half)):
+        def greet(p=p):
+            pl.semaphore_signal(barrier, inc=1, device_id=(group(p), tp), device_id_type=MESH)
+        if p == 0:
+            pl.when(core == 1)(greet)
+        else:
+            greet()
+    for d in range(1, planes):
+        pl.semaphore_signal(barrier, inc=1, device_id=(ep, 2 * lax.rem(y + d, planes) + core), device_id_type=MESH)
+    pl.semaphore_signal(barrier, inc=1, device_id=(ep, 2 * y + 1 - core), device_id_type=MESH)
 
     pairs = ((tokens_hbm, tokens), (gain_hbm, gain), (routing_hbm, routing), (route_weight_hbm, route_weight),
              (gate_hbm.at[0], gate.at[0:share]), (up_hbm.at[0], up.at[0:share]), (down_hbm.at[0], down.at[0:share]))
     loads = [pltpu.make_async_copy(source, target, load_sem.at[i]) for i, (source, target) in enumerate(pairs)]
     for i in (2, 3, 0, 1, 4, 5, 6):
         loads[i].start()
-
-    far_first = sorted(range(half), key=lambda q: -min(q, half - q))
-    barrier = pltpu.get_barrier_semaphore()
-    for q in far_first:
-        def greet(q=q):
-            pl.semaphore_signal(barrier, inc=1, device_id=(group(q), 2 * y + parity), device_id_type=MESH)
-        if q == 0:
-            pl.when(core != parity)(greet)
-        else:
-            greet()
-    for d in range(1, planes):
-        pl.semaphore_signal(barrier, inc=1, device_id=(ep, 2 * lax.rem(y + d, planes) + core), device_id_type=MESH)
-    pl.semaphore_signal(barrier, inc=1, device_id=(ep, 2 * y + 1 - core), device_id_type=MESH)
 
     count = tokens.shape[0]
     earlier = lax.broadcasted_iota(jnp.int32, (count, count), 0) < lax.broadcasted_iota(jnp.int32, (count, count), 1)
@@ -78,7 +92,13 @@
 
     loads[2].wait()
     loads[3].wait()
-    placed, _ = slots_of(rows, lambda q: group(q))
+
+    def named_at(line):
+        expert = jnp.zeros_like(line)
+        for p in range(half):
+            expert = jnp.where(line == p, group(p), expert)
+        return expert
+    placed, _ = slots_of(rows, named_at)
     loads[0].wait()
     loads[1].wait()
     values = tokens[...].astype(jnp.float32)
@@ -87,21 +107,19 @@
     sent = jnp.dot(placed.astype(jnp.bfloat16), normed, preferred_element_type=jnp.float32)
     outgoing[...] = sent.reshape(half, CAP, width).astype(jnp.bfloat16)
 
-    pl.semaphore_wait(barrier, half + planes - own)
-
-    for q in far_first:
-        at = position[(half - q) % half]
-
-        def dispatch(q=q, at=at):
+    pl.semaphore_wait(barrier, half + planes - 1 + core)
+
+    for p in reversed(range(half)):
+        def dispatch(p=p):
             pltpu.make_async_remote_copy(
-                src_ref=outgoing.at[q], dst_ref=incoming.at[at], send_sem=out_sem, recv_sem=in_sem.at[chunk_of[at]],
-                device_id=(group(q), 2 * y + parity), device_id_type=MESH).start()
-
-        def keep(q=q, at=at):
-            incoming[at] = outgoing[q]
-        if q == 0:
-            pl.when(core != parity)(dispatch)
-            pl.when(core == parity)(keep)
+                src_ref=outgoing.at[p], dst_ref=incoming.at[back_at[p]], send_sem=out_sem,
+                recv_sem=in_sem.at[chunk_of[back_at[p]]], device_id=(group(p), tp), device_id_type=MESH).start()
+
+        def keep(p=p):
+            incoming[p] = outgoing[p]
+        if p == 0:
+            pl.when(core == 1)(dispatch)
+            pl.when(core == 0)(keep)
         else:
             dispatch()
 
@@ -123,8 +141,8 @@
 
     def wait_for(ref, sem, most):
         less, full = ref.at[pl.ds(0, most - 1)], ref.at[pl.ds(0, most)]
-        pl.when(core == parity)(lambda: pltpu.make_async_copy(less, less, sem).wait())
-        pl.when(core != parity)(lambda: pltpu.make_async_copy(full, full, sem).wait())
+        pl.when(core == 0)(lambda: pltpu.make_async_copy(less, less, sem).wait())
+        pl.when(core == 1)(lambda: pltpu.make_async_copy(full, full, sem).wait())
 
     order = sorted(range(1, planes), key=lambda d: -min(d, planes - d))
     pieces = [piece for some in PIECES for piece in some]
@@ -194,14 +212,16 @@
                 def send(at=at, side=side):
                     pltpu.make_async_remote_copy(
                         src_ref=back.at[side, at], dst_ref=arrived.at[ep], send_sem=back_send, recv_sem=back_recv,
-                        device_id=(group(offset[at]), 2 * y + side), device_id_type=MESH).start()
+                        device_id=(group(at), 2 * y + side), device_id_type=MESH).start()
 
                 def hold(at=at, side=side):
                     arrived[ep] = back[side, at]
                 if at == 0:
-                    here = jnp.logical_and(core == parity, core == side)
-                    pl.when(here)(hold)
-                    pl.when(jnp.logical_not(here))(send)
+                    if side == 0:
+                        pl.when(core == 0)(hold)
+                        pl.when(core == 1)(send)
+                    else:
+                        send()
                 else:
                     send()
 

time: 33.5 us -> 33 us (0.985)
  Pallas kernels: 32.8 us -> 32.3 us
    pallas_call x1, Pallas kernels: 32.8 us -> 32.3 us  [local(): pl.pallas_call(functools.partial(kernel, groups, shares), out_shape=pltpu...]
where the time goes in v5:
time: 33 us
  Pallas kernels  32.3 us (98%)
  local copies, waits for them, and re-layouts  0.6 us (2%)
    pallas_call x1, Pallas kernels, local(): pl.pallas_call(functools.partial(kernel, groups, shares), out_shape=pltpu...  32.3 us

profile of v5, /device:TPU:1, one launch (start us, length us, event | category | flops | bytes accessed | tf_op | source)
XLA Modules:
  0.0 33.0 jit_solution(9967983009778508436)
XLA Ops:
  0.0 32.3 %experts.1 = bf16[16,128]{1,0:T(8,128)(2,1)S(1)} custom-call(bf16[16,1024]{1,0:T(8,128)(2,1)} %tokens_hbm.1, f32[1,1024]{1,0:T(1,128)} %bitcast.7, s32[2,16]{1,0:T(2,128)} %bitcast.8, f32[2,16]{1,0:T(2,128)} %bitcast.9, bf16[1,448,1024]{2,1,0:T(8,128)(2,1)} %bitcast.5, bf16[1,448,1024]{2,1,0:T(8,128)(2,1)} %bitcast.6, bf16[1,448,1024]{2,1,0:T(8,128)(2,1)} %down_hbm.1), custom_call_target="tpu_custom_call" | custom-call | tf_op jit(solution)/shard_map/experts/pallas_call | solution.py:258
  32.4 0.6 %copy.9 = bf16[16,128]{1,0:T(8,128)(2,1)} copy(bf16[16,128]{1,0:T(8,128)(2,1)S(1)} %experts.1) | data formatting | bytes 8192

commit v6 on v4

v6 whole, which is shorter than its diff:
```python
import functools

import jax
import jax.numpy as jnp
from jax import lax
from jax.experimental import pallas as pl
from jax.experimental.pallas import tpu as pltpu
from jax.sharding import PartitionSpec as P

CAP = 8
XS = 4
CHUNKS = ((0, 16),)
PIECES = (((0, 4, 1), (0, 4, 0), (4, 16, 1), (4, 16, 0)),)
STEPS = ('c0', 'r0', 'r1', 'r2', 'r3')
STEPS_16 = 32767.0
LEAST = 2e-34
MESH = pl.DeviceIdType.MESH

norm_eps = 1e-06


def kernel(groups, shares, tokens_hbm, gain_hbm, routing_hbm, route_weight_hbm, gate_hbm, up_hbm, down_hbm, mixed,
           tokens, gain, routing, route_weight, gate, up, down, gate_across, up_across,
           outgoing, incoming, partial, reduced, peak, their_peak, back, arrived,
           load_sem, swap_send, swap_recv, out_sem, in_sem, part_send, part_recv, peak_send, peak_recv, back_send, back_recv):
    ep, tp = lax.axis_index("ep"), lax.axis_index("tp")
    width = tokens.shape[1]
    part = mixed.shape[1]
    half = groups // 2
    rows = half * CAP
    planes = shares // 2
    share = gate_hbm.shape[1]
    y, core = tp // 2, lax.rem(tp, 2)
    zs = groups // XS
    z, x = ep // XS, lax.rem(ep, XS)
    lower = 1 - z // (zs // 2)
    theirs, goal = half * (1 - core), half * core

    def near(q, dx):
        return XS * lax.rem(z + q, zs // 2) + lax.rem(x + dx, XS)

    rounds = [(q, dx) for q in (0, 3, 1, 2) for dx in (2, 3, 1, 0)]

    chunk_of = {p: k for k, (first, upto) in enumerate(CHUNKS) for p in range(first, upto)}
    tile = 2 * part

    barrier = pltpu.get_barrier_semaphore()
    for q, dx in rounds:
        pl.semaphore_signal(barrier, inc=1, device_id=(theirs + near(q, dx), 2 * y + 1 - lower), device_id_type=MESH)
    for d in range(1, planes):
        pl.semaphore_signal(barrier, inc=1, device_id=(ep, 2 * lax.rem(y + d, planes) + core), device_id_type=MESH)
    pl.semaphore_signal(barrier, inc=1, device_id=(ep, 2 * y + 1 - core), device_id_type=MESH)

    pairs = ((tokens_hbm, tokens), (gain_hbm, gain), (routing_hbm, routing), (route_weight_hbm, route_weight),
             (gate_hbm.at[0], gate.at[0:share]), (up_hbm.at[0], up.at[0:share]), (down_hbm.at[0], down.at[0:share]))
    loads = [pltpu.make_async_copy(source, target, load_sem.at[i]) for i, (source, target) in enumerate(pairs)]
    for i in (2, 3, 0, 1, 4, 5, 6):
        loads[i].start()

    count = tokens.shape[0]
    earlier = lax.broadcasted_iota(jnp.int32, (count, count), 0) < lax.broadcasted_iota(jnp.int32, (count, count), 1)
    earlier = jnp.where(earlier, 1.0, 0.0).astype(jnp.bfloat16)

    def slots_of(lines, expert_of):
        line = lax.broadcasted_iota(jnp.int32, (lines, count), 0)
        expert = expert_of(line // CAP)
        member = jnp.zeros((lines, count), jnp.float32)
        weight = jnp.zeros((lines, count), jnp.float32)
        for k in range(routing.shape[0]):
            named = routing[k:k + 1, :] == expert
            member = jnp.where(named, 1.0, member)
            weight = jnp.where(named, route_weight[k:k + 1, :], weight)
        before = jnp.dot(member.astype(jnp.bfloat16), earlier, preferred_element_type=jnp.float32)
        placed = jnp.where(before == lax.rem(line, CAP).astype(jnp.float32), member, 0.0)
        return placed, weight

    loads[2].wait()
    loads[3].wait()
    placed, _ = slots_of(rows, lambda p: goal + p)
    loads[0].wait()
    loads[1].wait()
    values = tokens[...].astype(jnp.float32)
    scale = lax.rsqrt(jnp.mean(values * values, axis=-1, keepdims=True) + norm_eps)
    normed = (values * scale * gain[...]).astype(jnp.bfloat16)
    sent = jnp.dot(placed.astype(jnp.bfloat16), normed, preferred_element_type=jnp.float32)
    outgoing[...] = sent.reshape(half, CAP, width).astype(jnp.bfloat16)

    pl.semaphore_wait(barrier, half + planes)

    for q, dx in rounds:
        p = near(q, dx)
        pltpu.make_async_remote_copy(
            src_ref=outgoing.at[p], dst_ref=incoming.at[lax.rem(ep, half)], send_sem=out_sem, recv_sem=in_sem.at[0],
            device_id=(goal + p, 2 * y + lower), device_id_type=MESH).start()

    swaps = [pltpu.make_async_remote_copy(
        src_ref=ref.at[0:share], dst_ref=ref.at[share:2 * share], send_sem=swap_send.at[i], recv_sem=swap_recv.at[i],
        device_id=(ep, 2 * y + 1 - core), device_id_type=MESH) for i, ref in enumerate((gate, up, down))]
    for i in (4, 5, 6):
        loads[i].wait()
    for swap in swaps:
        swap.start()

    picked, weight = slots_of(groups * CAP, lambda q: q)
    weight = jnp.transpose(weight * picked)

    for swap in swaps:
        swap.wait_recv()
    gate_across[...] = jnp.transpose(gate[...])
    up_across[...] = jnp.transpose(up[...])

    def wait_for(ref, sem, most):
        less, full = ref.at[pl.ds(0, most - 1)], ref.at[pl.ds(0, most)]
        pl.when(core == lower)(lambda: pltpu.make_async_copy(less, less, sem).wait())
        pl.when(core != lower)(lambda: pltpu.make_async_copy(full, full, sem).wait())

    def wait_all(ref, sem):
        pltpu.make_async_copy(ref, ref, sem).wait()

    pieces = [piece for some in PIECES for piece in some]
    totals = {}
    others = range(planes - 1)

    def plane(d):
        return d + (d + planes - y) // planes

    def seen_at(d):
        return y - (y + planes - 1 - plane(d)) // planes

    def columns(to):
        return pl.ds(pl.multiple_of(to * tile, tile), tile)

    def give(d, piece):
        some, side, k = pl.ds(piece[0] * CAP, (piece[1] - piece[0]) * CAP), piece[2], pieces.index(piece)
        return pltpu.make_async_remote_copy(
            src_ref=partial.at[d, side, some], dst_ref=reduced.at[seen_at(d), side, some],
            send_sem=part_send.at[d, k], recv_sem=part_recv.at[seen_at(d), k],
            device_id=(ep, 2 * plane(d) + core), device_id_type=MESH)

    def received(d, piece):
        some, side, k = pl.ds(piece[0] * CAP, (piece[1] - piece[0]) * CAP), piece[2], pieces.index(piece)
        return pltpu.make_async_copy(reduced.at[d, side, some], reduced.at[d, side, some], part_recv.at[d, k])

    def give_peak(d):
        return pltpu.make_async_remote_copy(
            src_ref=peak.at[d], dst_ref=their_peak.at[seen_at(d)], send_sem=peak_send.at[d],
            recv_sem=peak_recv.at[seen_at(d)], device_id=(ep, 2 * plane(d) + core), device_id_type=MESH)

    def multiply(k):
        first, upto = CHUNKS[k]
        wait_all(incoming.at[pl.ds(first, upto - first)], in_sem.at[k])
        a = incoming[first:upto].astype(jnp.float32).reshape((upto - first) * CAP, width).astype(jnp.bfloat16)
        gate_act = jnp.dot(a, gate_across[...], preferred_element_type=jnp.float32)
        up_act = jnp.dot(a, up_across[...], preferred_element_type=jnp.float32)
        hidden = (gate_act / (1.0 + jnp.exp(-gate_act)) * up_act).astype(jnp.bfloat16)
        for d in others:
            block = jnp.dot(hidden, down[:, columns(plane(d))], preferred_element_type=jnp.float32)
            sides = [block[:, side * part:(side + 1) * part].reshape(upto - first, CAP, part) for side in range(2)]
            most = jnp.maximum(jnp.max(jnp.maximum(jnp.abs(sides[0]), jnp.abs(sides[1])), axis=0), LEAST)
            peak[d] = most
            give_peak(d).start()
            for side in range(2):
                coded = jnp.round(sides[side] * (STEPS_16 / most)).reshape((upto - first) * CAP, part)
                partial[d, side, first * CAP:upto * CAP] = (
                    coded.astype(jnp.int32).astype(jnp.int16))
            give(d, PIECES[k][0]).start()
        for piece in PIECES[k][1:]:
            for d in others:
                give(d, piece).start()
        mine = jnp.dot(hidden, down[:, columns(y)], preferred_element_type=jnp.float32)
        for piece in PIECES[k]:
            totals[piece] = mine[(piece[0] - first) * CAP:(piece[1] - first) * CAP]

    def give_back(k):
        piece = pieces[k]
        first, upto, side = piece
        for d in others:
            if k == 0:
                pltpu.make_async_copy(their_peak.at[d], their_peak.at[d], peak_recv.at[d]).wait()
            received(d, piece).wait()
        total = totals[piece][:, side * part:(side + 1) * part].reshape(upto - first, CAP, part)
        for d in others:
            coded = reduced[d, side, first * CAP:upto * CAP].astype(jnp.int32).astype(jnp.float32)
            total = total + coded.reshape(upto - first, CAP, part) * (their_peak[d] * (1.0 / STEPS_16))
        back[side, first:upto] = total
        for start in range(first, upto, XS):
            for dx in (2, 3, 1, 0):
                p = start + lax.rem(x + dx, XS)

                def send(p=p):
                    pltpu.make_async_remote_copy(
                        src_ref=back.at[side, p], dst_ref=arrived.at[ep], send_sem=back_send, recv_sem=back_recv,
                        device_id=(theirs + p, 2 * y + side), device_id_type=MESH).start()

                def hold(p=p):
                    arrived[ep] = back[side, p]
                if dx == 0:
                    here = jnp.logical_and(theirs + p == ep, core == side)
                    pl.when(here)(hold)
                    pl.when(jnp.logical_not(here))(send)
                else:
                    send()

    for step in STEPS:
        (multiply if step[0] == "c" else give_back)(int(step[1:]))

    wait_for(arrived, back_recv, groups)
    out = jnp.dot(weight, arrived[...].reshape(groups * CAP, part), precision=lax.Precision.HIGHEST,
                  preferred_element_type=jnp.float32)
    mixed[...] = out.astype(mixed.dtype)
    wait_all(outgoing, out_sem)
    for swap in swaps:
        swap.wait_send()
    for d in others:
        give_peak(d).wait_send()
    for piece in pieces:
        for d in others:
            give(d, piece).wait_send()
    wait_for(arrived, back_send, groups)


def solution(mesh):
    groups, shares = mesh.shape["ep"], mesh.shape["tp"]

    def local(tokens, norm_gain, routing, route_weight, w_gate, w_up, w_down):
        count, width = tokens.shape
        part = width // shares
        half, planes = groups // 2, shares // 2
        rows = half * CAP
        share = w_down.shape[1]
        pieces = sum(map(len, PIECES))
        vmem = pl.BlockSpec(memory_space=pltpu.VMEM)
        hbm = pl.BlockSpec(memory_space=pltpu.HBM)
        return pl.pallas_call(
            functools.partial(kernel, groups, shares),
            out_shape=pltpu.VMEM((count, part), jnp.bfloat16),
            in_specs=[hbm] * 7,
            out_specs=vmem,
            scratch_shapes=[
                pltpu.VMEM((count, width), tokens.dtype),
                pltpu.VMEM((1, width), norm_gain.dtype),
                pltpu.VMEM(routing.shape[::-1], routing.dtype),
                pltpu.VMEM(route_weight.shape[::-1], route_weight.dtype),
                pltpu.VMEM((2 * share, width), jnp.bfloat16),
                pltpu.VMEM((2 * share, width), jnp.bfloat16),
                pltpu.VMEM((2 * share, width), jnp.bfloat16),
                pltpu.VMEM((width, 2 * share), jnp.bfloat16),
                pltpu.VMEM((width, 2 * share), jnp.bfloat16),
                pltpu.VMEM((half, CAP, width), jnp.bfloat16),
                pltpu.VMEM((half, CAP, width), jnp.bfloat16),
                pltpu.VMEM((planes - 1, 2, rows, part), jnp.int16),
                pltpu.VMEM((planes - 1, 2, rows, part), jnp.int16),
                pltpu.VMEM((planes - 1, CAP, part), jnp.float32),
                pltpu.VMEM((planes - 1, CAP, part), jnp.float32),
                pltpu.VMEM((2, half, CAP, part), jnp.float32),
                pltpu.VMEM((groups, CAP, part), jnp.float32),
                pltpu.SemaphoreType.DMA((7,)),
                pltpu.SemaphoreType.DMA((3,)),
                pltpu.SemaphoreType.DMA((3,)),
                pltpu.SemaphoreType.DMA,
                pltpu.SemaphoreType.DMA((len(CHUNKS),)),
                pltpu.SemaphoreType.DMA((planes - 1, pieces)),
                pltpu.SemaphoreType.DMA((planes - 1, pieces)),
                pltpu.SemaphoreType.DMA((planes - 1,)),
                pltpu.SemaphoreType.DMA((planes - 1,)),
                pltpu.SemaphoreType.DMA,
                pltpu.SemaphoreType.DMA,
            ],
            compiler_params=pltpu.CompilerParams(collective_id=0, has_side_effects=True,
                                                 vmem_limit_bytes=67043328 - 16384),
            name="experts",
        )(tokens, norm_gain.reshape(1, width), routing.T, route_weight.T,
          jnp.swapaxes(w_gate, 1, 2), jnp.swapaxes(w_up, 1, 2), w_down)

    in_specs = (
        P("ep", None),
        P(),
        P("ep", None),
        P("ep", None),
        P("ep", None, "tp"),
        P("ep", None, "tp"),
        P("ep", "tp", None),
    )
    return jax.shard_map(local, mesh=mesh, in_specs=in_specs, out_specs=P("ep", "tp"), check_vma=False)
```

time: 33.5 us -> 31.2 us (0.931)
  Pallas kernels: 32.8 us -> 30.3 us
    pallas_call x1, Pallas kernels: 32.8 us -> 30.3 us  [local(): pl.pallas_call(functools.partial(kernel, groups, shares), out_shape=pltpu...]
where the time goes in v6:
time: 31.2 us; the launch traced here: 30.9 us
  Pallas kernels  30.3 us (97%)
  local copies, waits for them, and re-layouts  0.6 us (2%)
    pallas_call x1, Pallas kernels, local(): pl.pallas_call(functools.partial(kernel, groups, shares), out_shape=pltpu...  30.3 us

profile of v6, /device:TPU:1, one launch (start us, length us, event | category | flops | bytes accessed | tf_op | source)
XLA Modules:
  0.0 30.9 jit_solution(17227065801727736802)
XLA Ops:
  0.0 30.3 %experts.1 = bf16[16,128]{1,0:T(8,128)(2,1)S(1)} custom-call(bf16[16,1024]{1,0:T(8,128)(2,1)} %tokens_hbm.1, f32[1,1024]{1,0:T(1,128)} %bitcast.7, s32[2,16]{1,0:T(2,128)} %bitcast.8, f32[2,16]{1,0:T(2,128)} %bitcast.9, bf16[1,448,1024]{2,1,0:T(8,128)(2,1)} %bitcast.5, bf16[1,448,1024]{2,1,0:T(8,128)(2,1)} %bitcast.6, bf16[1,448,1024]{2,1,0:T(8,128)(2,1)} %down_hbm.1), custom_call_target="tpu_custom_call" | custom-call | tf_op jit(solution)/shard_map/experts/pallas_call | solution.py:234
  30.3 0.6 %copy.9 = bf16[16,128]{1,0:T(8,128)(2,1)} copy(bf16[16,128]{1,0:T(8,128)(2,1)S(1)} %experts.1) | data formatting | bytes 8192

commit v7 on v6

--- a/solution.py
+++ b/solution.py
@@ -10,8 +10,8 @@
 CAP = 8
 XS = 4
 CHUNKS = ((0, 16),)
-PIECES = (((0, 4, 1), (0, 4, 0), (4, 16, 1), (4, 16, 0)),)
-STEPS = ('c0', 'r0', 'r1', 'r2', 'r3')
+PIECES = (((0, 4, 1), (0, 8, 0), (4, 12, 1), (8, 16, 0), (12, 16, 1)),)
+STEPS = ('c0', 'r0', 'r1', 'r2', 'r3', 'r4')
 STEPS_16 = 32767.0
 LEAST = 2e-34
 MESH = pl.DeviceIdType.MESH
@@ -39,7 +39,7 @@
     def near(q, dx):
         return XS * lax.rem(z + q, zs // 2) + lax.rem(x + dx, XS)
 
-    rounds = [(q, dx) for q in (0, 3, 1, 2) for dx in (2, 3, 1, 0)]
+    rounds = [(q, dx) for dx in (2, 3, 1, 0) for q in (0, 3, 1, 2)]
 
     chunk_of = {p: k for k, (first, upto) in enumerate(CHUNKS) for p in range(first, upto)}
     tile = 2 * part
@@ -87,11 +87,14 @@
 
     pl.semaphore_wait(barrier, half + planes)
 
-    for q, dx in rounds:
-        p = near(q, dx)
-        pltpu.make_async_remote_copy(
-            src_ref=outgoing.at[p], dst_ref=incoming.at[lax.rem(ep, half)], send_sem=out_sem, recv_sem=in_sem.at[0],
-            device_id=(goal + p, 2 * y + lower), device_id_type=MESH).start()
+    def dispatch():
+        for q, dx in rounds:
+            p = near(q, dx)
+            pltpu.make_async_remote_copy(
+                src_ref=outgoing.at[p], dst_ref=incoming.at[lax.rem(ep, half)], send_sem=out_sem, recv_sem=in_sem.at[0],
+                device_id=(goal + p, 2 * y + lower), device_id_type=MESH).start()
+
+    pl.when(lower + 1 - core > 0)(dispatch)
 
     swaps = [pltpu.make_async_remote_copy(
         src_ref=ref.at[0:share], dst_ref=ref.at[share:2 * share], send_sem=swap_send.at[i], recv_sem=swap_recv.at[i],
@@ -106,6 +109,7 @@
 
     for swap in swaps:
         swap.wait_recv()
+    pl.when(lower + 1 - core == 0)(dispatch)
     gate_across[...] = jnp.transpose(gate[...])
     up_across[...] = jnp.transpose(up[...])
 

time: 31.2 us -> 30 us (0.962)
  Pallas kernels: 30.3 us -> 29.3 us
    pallas_call x1, Pallas kernels: 30.3 us -> 29.3 us  [local(): pl.pallas_call(functools.partial(kernel, groups, shares), out_shape=pltpu...]
where the time goes in v7:
time: 30 us; the launch traced here: 29.9 us
  Pallas kernels  29.3 us (98%)
  local copies, waits for them, and re-layouts  0.6 us (2%)
    pallas_call x1, Pallas kernels, local(): pl.pallas_call(functools.partial(kernel, groups, shares), out_shape=pltpu...  29.3 us

profile of v7, /device:TPU:1, one launch (start us, length us, event | category | flops | bytes accessed | tf_op | source)
XLA Modules:
  0.0 29.9 jit_solution(5101606238191132068)
XLA Ops:
  0.0 29.3 %experts.1 = bf16[16,128]{1,0:T(8,128)(2,1)S(1)} custom-call(bf16[16,1024]{1,0:T(8,128)(2,1)} %tokens_hbm.1, f32[1,1024]{1,0:T(1,128)} %bitcast.7, s32[2,16]{1,0:T(2,128)} %bitcast.8, f32[2,16]{1,0:T(2,128)} %bitcast.9, bf16[1,448,1024]{2,1,0:T(8,128)(2,1)} %bitcast.5, bf16[1,448,1024]{2,1,0:T(8,128)(2,1)} %bitcast.6, bf16[1,448,1024]{2,1,0:T(8,128)(2,1)} %down_hbm.1), custom_call_target="tpu_custom_call" | custom-call | tf_op jit(solution)/shard_map/experts/pallas_call | solution.py:238
  29.3 0.6 %copy.9 = bf16[16,128]{1,0:T(8,128)(2,1)} copy(bf16[16,128]{1,0:T(8,128)(2,1)S(1)} %experts.1) | data formatting | bytes 8192

commit v8 on v7

--- a/solution.py
+++ b/solution.py
@@ -10,10 +10,8 @@
 CAP = 8
 XS = 4
 CHUNKS = ((0, 16),)
-PIECES = (((0, 4, 1), (0, 8, 0), (4, 12, 1), (8, 16, 0), (12, 16, 1)),)
-STEPS = ('c0', 'r0', 'r1', 'r2', 'r3', 'r4')
-STEPS_16 = 32767.0
-LEAST = 2e-34
+PIECES = (((0, 8, 1), (8, 12, 1), (0, 8, 0), (12, 16, 1), (8, 12, 0), (12, 16, 0)),)
+STEPS = ('c0', 'r0', 'r1', 'r2', 'r3', 'r4', 'r5')
 MESH = pl.DeviceIdType.MESH
 
 norm_eps = 1e-06
@@ -21,8 +19,8 @@
 
 def kernel(groups, shares, tokens_hbm, gain_hbm, routing_hbm, route_weight_hbm, gate_hbm, up_hbm, down_hbm, mixed,
            tokens, gain, routing, route_weight, gate, up, down, gate_across, up_across,
-           outgoing, incoming, partial, reduced, peak, their_peak, back, arrived,
-           load_sem, swap_send, swap_recv, out_sem, in_sem, part_send, part_recv, peak_send, peak_recv, back_send, back_recv):
+           outgoing, incoming, partial, reduced, back, arrived,
+           load_sem, swap_send, swap_recv, out_sem, in_sem, part_send, part_recv, back_send, back_recv):
     ep, tp = lax.axis_index("ep"), lax.axis_index("tp")
     width = tokens.shape[1]
     part = mixed.shape[1]
@@ -45,8 +43,8 @@
     tile = 2 * part
 
     barrier = pltpu.get_barrier_semaphore()
-    for q, dx in rounds:
-        pl.semaphore_signal(barrier, inc=1, device_id=(theirs + near(q, dx), 2 * y + 1 - lower), device_id_type=MESH)
+    for p in range(half):
+        pl.semaphore_signal(barrier, inc=1, device_id=(theirs + p, 2 * y + 1 - lower), device_id_type=MESH)
     for d in range(1, planes):
         pl.semaphore_signal(barrier, inc=1, device_id=(ep, 2 * lax.rem(y + d, planes) + core), device_id_type=MESH)
     pl.semaphore_signal(barrier, inc=1, device_id=(ep, 2 * y + 1 - core), device_id_type=MESH)
@@ -145,11 +143,6 @@
         some, side, k = pl.ds(piece[0] * CAP, (piece[1] - piece[0]) * CAP), piece[2], pieces.index(piece)
         return pltpu.make_async_copy(reduced.at[d, side, some], reduced.at[d, side, some], part_recv.at[d, k])
 
-    def give_peak(d):
-        return pltpu.make_async_remote_copy(
-            src_ref=peak.at[d], dst_ref=their_peak.at[seen_at(d)], send_sem=peak_send.at[d],
-            recv_sem=peak_recv.at[seen_at(d)], device_id=(ep, 2 * plane(d) + core), device_id_type=MESH)
-
     def multiply(k):
         first, upto = CHUNKS[k]
         wait_all(incoming.at[pl.ds(first, upto - first)], in_sem.at[k])
@@ -159,14 +152,8 @@
         hidden = (gate_act / (1.0 + jnp.exp(-gate_act)) * up_act).astype(jnp.bfloat16)
         for d in others:
             block = jnp.dot(hidden, down[:, columns(plane(d))], preferred_element_type=jnp.float32)
-            sides = [block[:, side * part:(side + 1) * part].reshape(upto - first, CAP, part) for side in range(2)]
-            most = jnp.maximum(jnp.max(jnp.maximum(jnp.abs(sides[0]), jnp.abs(sides[1])), axis=0), LEAST)
-            peak[d] = most
-            give_peak(d).start()
             for side in range(2):
-                coded = jnp.round(sides[side] * (STEPS_16 / most)).reshape((upto - first) * CAP, part)
-                partial[d, side, first * CAP:upto * CAP] = (
-                    coded.astype(jnp.int32).astype(jnp.int16))
+                partial[d, side, first * CAP:upto * CAP] = block[:, side * part:(side + 1) * part]
             give(d, PIECES[k][0]).start()
         for piece in PIECES[k][1:]:
             for d in others:
@@ -179,13 +166,10 @@
         piece = pieces[k]
         first, upto, side = piece
         for d in others:
-            if k == 0:
-                pltpu.make_async_copy(their_peak.at[d], their_peak.at[d], peak_recv.at[d]).wait()
             received(d, piece).wait()
         total = totals[piece][:, side * part:(side + 1) * part].reshape(upto - first, CAP, part)
         for d in others:
-            coded = reduced[d, side, first * CAP:upto * CAP].astype(jnp.int32).astype(jnp.float32)
-            total = total + coded.reshape(upto - first, CAP, part) * (their_peak[d] * (1.0 / STEPS_16))
+            total = total + reduced[d, side, first * CAP:upto * CAP].reshape(upto - first, CAP, part)
         back[side, first:upto] = total
         for start in range(first, upto, XS):
             for dx in (2, 3, 1, 0):
@@ -215,8 +199,6 @@
     wait_all(outgoing, out_sem)
     for swap in swaps:
         swap.wait_send()
-    for d in others:
-        give_peak(d).wait_send()
     for piece in pieces:
         for d in others:
             give(d, piece).wait_send()
@@ -252,10 +234,8 @@
                 pltpu.VMEM((width, 2 * share), jnp.bfloat16),
                 pltpu.VMEM((half, CAP, width), jnp.bfloat16),
                 pltpu.VMEM((half, CAP, width), jnp.bfloat16),
-                pltpu.VMEM((planes - 1, 2, rows, part), jnp.int16),
-                pltpu.VMEM((planes - 1, 2, rows, part), jnp.int16),
-                pltpu.VMEM((planes - 1, CAP, part), jnp.float32),
-                pltpu.VMEM((planes - 1, CAP, part), jnp.float32),
+                pltpu.VMEM((planes - 1, 2, rows, part), jnp.float32),
+                pltpu.VMEM((planes - 1, 2, rows, part), jnp.float32),
                 pltpu.VMEM((2, half, CAP, part), jnp.float32),
                 pltpu.VMEM((groups, CAP, part), jnp.float32),
                 pltpu.SemaphoreType.DMA((7,)),
@@ -265,8 +245,6 @@
                 pltpu.SemaphoreType.DMA((len(CHUNKS),)),
                 pltpu.SemaphoreType.DMA((planes - 1, pieces)),
                 pltpu.SemaphoreType.DMA((planes - 1, pieces)),
-                pltpu.SemaphoreType.DMA((planes - 1,)),
-                pltpu.SemaphoreType.DMA((planes - 1,)),
                 pltpu.SemaphoreType.DMA,
                 pltpu.SemaphoreType.DMA,
             ],

time: 30 us -> 30.9 us (1.030)
  the two profiles are of different devices: /device:TPU:1 before, /device:TPU:64 now
where the time goes in v8:
time: 30.9 us; the launch traced here: 30.8 us
  Pallas kernels  30.2 us (98%)
  local copies, waits for them, and re-layouts  0.6 us (2%)
    pallas_call x1, Pallas kernels, local(): pl.pallas_call(functools.partial(kernel, groups, shares), out_shape=pltpu...  30.2 us

profile of v8, /device:TPU:64, one launch (start us, length us, event | category | flops | bytes accessed | tf_op | source)
XLA Modules:
  0.0 30.8 jit_solution(6259429907867055826)
XLA Ops:
  0.0 30.2 %experts.1 = bf16[16,128]{1,0:T(8,128)(2,1)S(1)} custom-call(bf16[16,1024]{1,0:T(8,128)(2,1)} %tokens_hbm.1, f32[1,1024]{1,0:T(1,128)} %bitcast.7, s32[2,16]{1,0:T(2,128)} %bitcast.8, f32[2,16]{1,0:T(2,128)} %bitcast.9, bf16[1,448,1024]{2,1,0:T(8,128)(2,1)} %bitcast.5, bf16[1,448,1024]{2,1,0:T(8,128)(2,1)} %bitcast.6, bf16[1,448,1024]{2,1,0:T(8,128)(2,1)} %down_hbm.1), custom_call_target="tpu_custom_call" | custom-call | tf_op jit(solution)/shard_map/experts/pallas_call | solution.py:220
  30.2 0.6 %copy.9 = bf16[16,128]{1,0:T(8,128)(2,1)} copy(bf16[16,128]{1,0:T(8,128)(2,1)S(1)} %experts.1) | data formatting | bytes 8192

commit v9 on v7

--- a/solution.py
+++ b/solution.py
@@ -10,8 +10,8 @@
 CAP = 8
 XS = 4
 CHUNKS = ((0, 16),)
-PIECES = (((0, 4, 1), (0, 8, 0), (4, 12, 1), (8, 16, 0), (12, 16, 1)),)
-STEPS = ('c0', 'r0', 'r1', 'r2', 'r3', 'r4')
+PIECES = (((0, 4, 1), (0, 8, 0), (4, 16, 1), (8, 16, 0)),)
+STEPS = ('c0', 'r0', 'r1', 'r2', 'r3')
 STEPS_16 = 32767.0
 LEAST = 2e-34
 MESH = pl.DeviceIdType.MESH
@@ -21,8 +21,8 @@
 
 def kernel(groups, shares, tokens_hbm, gain_hbm, routing_hbm, route_weight_hbm, gate_hbm, up_hbm, down_hbm, mixed,
            tokens, gain, routing, route_weight, gate, up, down, gate_across, up_across,
-           outgoing, incoming, partial, reduced, peak, their_peak, back, arrived,
-           load_sem, swap_send, swap_recv, out_sem, in_sem, part_send, part_recv, peak_send, peak_recv, back_send, back_recv):
+           outgoing, helping, incoming, partial, reduced, peak, their_peak, back, arrived,
+           load_sem, swap_send, swap_recv, out_sem, help_sem, in_sem, part_send, part_recv, peak_send, peak_recv, back_send, back_recv):
     ep, tp = lax.axis_index("ep"), lax.axis_index("tp")
     width = tokens.shape[1]
     part = mixed.shape[1]
@@ -45,8 +45,11 @@
     tile = 2 * part
 
     barrier = pltpu.get_barrier_semaphore()
+    closer = [(q, dx) for q, dx in rounds if q == 2]
+    cross = jnp.logical_and(lower == 0, core == 1).astype(jnp.int32)
     for q, dx in rounds:
-        pl.semaphore_signal(barrier, inc=1, device_id=(theirs + near(q, dx), 2 * y + 1 - lower), device_id_type=MESH)
+        other = 1 - lower - cross if (q, dx) in closer else 1 - lower
+        pl.semaphore_signal(barrier, inc=1, device_id=(theirs + near(q, dx), 2 * y + other), device_id_type=MESH)
     for d in range(1, planes):
         pl.semaphore_signal(barrier, inc=1, device_id=(ep, 2 * lax.rem(y + d, planes) + core), device_id_type=MESH)
     pl.semaphore_signal(barrier, inc=1, device_id=(ep, 2 * y + 1 - core), device_id_type=MESH)
@@ -84,16 +87,38 @@
     normed = (values * scale * gain[...]).astype(jnp.bfloat16)
     sent = jnp.dot(placed.astype(jnp.bfloat16), normed, preferred_element_type=jnp.float32)
     outgoing[...] = sent.reshape(half, CAP, width).astype(jnp.bfloat16)
-
-    pl.semaphore_wait(barrier, half + planes)
+    helps = jnp.logical_and(lower == 1, core == 0)
+
+    @pl.when(helps)
+    def _():
+        more, _ = slots_of(rows, lambda p: half + p)
+        sent = jnp.dot(more.astype(jnp.bfloat16), normed, preferred_element_type=jnp.float32)
+        helping[...] = sent.reshape(half, CAP, width).astype(jnp.bfloat16)
+
+    pl.semaphore_wait(barrier, half + planes + len(closer) * lower * (1 - 2 * core))
+
+    def send_block(block, sem, expert):
+        pltpu.make_async_remote_copy(
+            src_ref=block, dst_ref=incoming.at[lax.rem(ep, half)], send_sem=sem, recv_sem=in_sem.at[0],
+            device_id=(expert, 2 * y + lower), device_id_type=MESH).start()
+
+    def help_out():
+        for q, dx in closer:
+            p = near(q, dx)
+            send_block(helping.at[p], help_sem, half + p)
+
+    keeps = jnp.logical_or(lower == 0, core == 0)
 
     def dispatch():
         for q, dx in rounds:
-            p = near(q, dx)
-            pltpu.make_async_remote_copy(
-                src_ref=outgoing.at[p], dst_ref=incoming.at[lax.rem(ep, half)], send_sem=out_sem, recv_sem=in_sem.at[0],
-                device_id=(goal + p, 2 * y + lower), device_id_type=MESH).start()
-
+            def send(p=near(q, dx)):
+                send_block(outgoing.at[p], out_sem, goal + p)
+            if (q, dx) in closer:
+                pl.when(keeps)(send)
+            else:
+                send()
+
+    pl.when(helps)(help_out)
     pl.when(lower + 1 - core > 0)(dispatch)
 
     swaps = [pltpu.make_async_remote_copy(
@@ -212,7 +237,12 @@
     out = jnp.dot(weight, arrived[...].reshape(groups * CAP, part), precision=lax.Precision.HIGHEST,
                   preferred_element_type=jnp.float32)
     mixed[...] = out.astype(mixed.dtype)
-    wait_all(outgoing, out_sem)
+    def wait_some(ref, blocks, sem):
+        some = ref.at[pl.ds(0, blocks)]
+        pltpu.make_async_copy(some, some, sem).wait()
+    pl.when(keeps)(lambda: wait_some(outgoing, half, out_sem))
+    pl.when(jnp.logical_not(keeps))(lambda: wait_some(outgoing, half - len(closer), out_sem))
+    pl.when(helps)(lambda: wait_some(helping, len(closer), help_sem))
     for swap in swaps:
         swap.wait_send()
     for d in others:
@@ -252,6 +282,7 @@
                 pltpu.VMEM((width, 2 * share), jnp.bfloat16),
                 pltpu.VMEM((half, CAP, width), jnp.bfloat16),
                 pltpu.VMEM((half, CAP, width), jnp.bfloat16),
+                pltpu.VMEM((half, CAP, width), jnp.bfloat16),
                 pltpu.VMEM((planes - 1, 2, rows, part), jnp.int16),
                 pltpu.VMEM((planes - 1, 2, rows, part), jnp.int16),
                 pltpu.VMEM((planes - 1, CAP, part), jnp.float32),
@@ -261,6 +292,7 @@
                 pltpu.SemaphoreType.DMA((7,)),
                 pltpu.SemaphoreType.DMA((3,)),
                 pltpu.SemaphoreType.DMA((3,)),
+                pltpu.SemaphoreType.DMA,
                 pltpu.SemaphoreType.DMA,
                 pltpu.SemaphoreType.DMA((len(CHUNKS),)),
                 pltpu.SemaphoreType.DMA((planes - 1, pieces)),

time: 30 us -> 29.4 us (0.980)
  Pallas kernels: 29.3 us -> 28.6 us
    pallas_call x1, Pallas kernels: 29.3 us -> 28.6 us  [local(): pl.pallas_call(functools.partial(kernel, groups, shares), out_shape=pltpu...]
where the time goes in v9:
time: 29.4 us; the launch traced here: 29.2 us
  Pallas kernels  28.6 us (97%)
  local copies, waits for them, and re-layouts  0.6 us (2%)
    pallas_call x1, Pallas kernels, local(): pl.pallas_call(functools.partial(kernel, groups, shares), out_shape=pltpu...  28.6 us
    unnamed x1, local copies, waits for them, and re-layouts  0.6 us

profile of v9, /device:TPU:1, one launch (start us, length us, event | category | flops | bytes accessed | tf_op | source)
XLA Modules:
  0.0 29.2 jit_solution(2106676463292203533)
XLA Ops:
  0.0 28.6 %experts.1 = bf16[16,128]{1,0:T(8,128)(2,1)S(1)} custom-call(bf16[16,1024]{1,0:T(8,128)(2,1)} %tokens_hbm.1, f32[1,1024]{1,0:T(1,128)} %bitcast.7, s32[2,16]{1,0:T(2,128)} %bitcast.8, f32[2,16]{1,0:T(2,128)} %bitcast.9, bf16[1,448,1024]{2,1,0:T(8,128)(2,1)} %bitcast.5, bf16[1,448,1024]{2,1,0:T(8,128)(2,1)} %bitcast.6, bf16[1,448,1024]{2,1,0:T(8,128)(2,1)} %down_hbm.1), custom_call_target="tpu_custom_call" | custom-call | tf_op jit(solution)/shard_map/experts/pallas_call | solution.py:268
  28.6 0.6 %copy.9 = bf16[16,128]{1,0:T(8,128)(2,1)} copy(bf16[16,128]{1,0:T(8,128)(2,1)S(1)} %experts.1) | data formatting | bytes 8192

commit v10 on v9

--- a/solution.py
+++ b/solution.py
@@ -39,7 +39,7 @@
     def near(q, dx):
         return XS * lax.rem(z + q, zs // 2) + lax.rem(x + dx, XS)
 
-    rounds = [(q, dx) for dx in (2, 3, 1, 0) for q in (0, 3, 1, 2)]
+    rounds = [(q, dx) for dx in (2, 3, 1, 0) for q in (0, 1, 3, 2)]
 
     chunk_of = {p: k for k, (first, upto) in enumerate(CHUNKS) for p in range(first, upto)}
     tile = 2 * part
@@ -213,7 +213,7 @@
             total = total + coded.reshape(upto - first, CAP, part) * (their_peak[d] * (1.0 / STEPS_16))
         back[side, first:upto] = total
         for start in range(first, upto, XS):
-            for dx in (2, 3, 1, 0):
+            for dx in (2, 1, 3, 0):
                 p = start + lax.rem(x + dx, XS)
 
                 def send(p=p):

time: 29.4 us -> 29.2 us (level)
  no operation moved by 1% of the time
where the time goes in v10:
time: 29.2 us; the launch traced here: 29.1 us
  Pallas kernels  28.5 us (98%)
  local copies, waits for them, and re-layouts  0.6 us (2%)
    pallas_call x1, Pallas kernels, local(): pl.pallas_call(functools.partial(kernel, groups, shares), out_shape=pltpu...  28.5 us
    unnamed x1, local copies, waits for them, and re-layouts  0.6 us

profile of v10, /device:TPU:1, one launch (start us, length us, event | category | flops | bytes accessed | tf_op | source)
XLA Modules:
  0.0 29.1 jit_solution(5225147150316714570)
XLA Ops:
  0.0 28.5 %experts.1 = bf16[16,128]{1,0:T(8,128)(2,1)S(1)} custom-call(bf16[16,1024]{1,0:T(8,128)(2,1)} %tokens_hbm.1, f32[1,1024]{1,0:T(1,128)} %bitcast.7, s32[2,16]{1,0:T(2,128)} %bitcast.8, f32[2,16]{1,0:T(2,128)} %bitcast.9, bf16[1,448,1024]{2,1,0:T(8,128)(2,1)} %bitcast.5, bf16[1,448,1024]{2,1,0:T(8,128)(2,1)} %bitcast.6, bf16[1,448,1024]{2,1,0:T(8,128)(2,1)} %down_hbm.1), custom_call_target="tpu_custom_call" | custom-call | tf_op jit(solution)/shard_map/experts/pallas_call | solution.py:268
  28.5 0.6 %copy.9 = bf16[16,128]{1,0:T(8,128)(2,1)} copy(bf16[16,128]{1,0:T(8,128)(2,1)S(1)} %experts.1) | data formatting | bytes 8192

commit v11 on v10

--- a/solution.py
+++ b/solution.py
@@ -10,10 +10,8 @@
 CAP = 8
 XS = 4
 CHUNKS = ((0, 16),)
-PIECES = (((0, 4, 1), (0, 8, 0), (4, 16, 1), (8, 16, 0)),)
-STEPS = ('c0', 'r0', 'r1', 'r2', 'r3')
-STEPS_16 = 32767.0
-LEAST = 2e-34
+PIECES = (((0, 8, 1), (8, 12, 1), (0, 8, 0), (8, 12, 0), (12, 16, 1), (12, 16, 0)),)
+STEPS = ('c0', 'r0', 'r1', 'r2', 'r3', 'r4', 'r5')
 MESH = pl.DeviceIdType.MESH
 
 norm_eps = 1e-06
@@ -21,8 +19,8 @@
 
 def kernel(groups, shares, tokens_hbm, gain_hbm, routing_hbm, route_weight_hbm, gate_hbm, up_hbm, down_hbm, mixed,
            tokens, gain, routing, route_weight, gate, up, down, gate_across, up_across,
-           outgoing, helping, incoming, partial, reduced, peak, their_peak, back, arrived,
-           load_sem, swap_send, swap_recv, out_sem, help_sem, in_sem, part_send, part_recv, peak_send, peak_recv, back_send, back_recv):
+           outgoing, helping, incoming, partial, reduced, back, arrived,
+           load_sem, swap_send, swap_recv, out_sem, help_sem, in_sem, part_send, part_recv, back_send, back_recv):
     ep, tp = lax.axis_index("ep"), lax.axis_index("tp")
     width = tokens.shape[1]
     part = mixed.shape[1]
@@ -170,11 +168,6 @@
         some, side, k = pl.ds(piece[0] * CAP, (piece[1] - piece[0]) * CAP), piece[2], pieces.index(piece)
         return pltpu.make_async_copy(reduced.at[d, side, some], reduced.at[d, side, some], part_recv.at[d, k])
 
-    def give_peak(d):
-        return pltpu.make_async_remote_copy(
-            src_ref=peak.at[d], dst_ref=their_peak.at[seen_at(d)], send_sem=peak_send.at[d],
-            recv_sem=peak_recv.at[seen_at(d)], device_id=(ep, 2 * plane(d) + core), device_id_type=MESH)
-
     def multiply(k):
         first, upto = CHUNKS[k]
         wait_all(incoming.at[pl.ds(first, upto - first)], in_sem.at[k])
@@ -184,14 +177,8 @@
         hidden = (gate_act / (1.0 + jnp.exp(-gate_act)) * up_act).astype(jnp.bfloat16)
         for d in others:
             block = jnp.dot(hidden, down[:, columns(plane(d))], preferred_element_type=jnp.float32)
-            sides = [block[:, side * part:(side + 1) * part].reshape(upto - first, CAP, part) for side in range(2)]
-            most = jnp.maximum(jnp.max(jnp.maximum(jnp.abs(sides[0]), jnp.abs(sides[1])), axis=0), LEAST)
-            peak[d] = most
-            give_peak(d).start()
             for side in range(2):
-                coded = jnp.round(sides[side] * (STEPS_16 / most)).reshape((upto - first) * CAP, part)
-                partial[d, side, first * CAP:upto * CAP] = (
-                    coded.astype(jnp.int32).astype(jnp.int16))
+                partial[d, side, first * CAP:upto * CAP] = block[:, side * part:(side + 1) * part]
             give(d, PIECES[k][0]).start()
         for piece in PIECES[k][1:]:
             for d in others:
@@ -204,13 +191,10 @@
         piece = pieces[k]
         first, upto, side = piece
         for d in others:
-            if k == 0:
-                pltpu.make_async_copy(their_peak.at[d], their_peak.at[d], peak_recv.at[d]).wait()
             received(d, piece).wait()
         total = totals[piece][:, side * part:(side + 1) * part].reshape(upto - first, CAP, part)
         for d in others:
-            coded = reduced[d, side, first * CAP:upto * CAP].astype(jnp.int32).astype(jnp.float32)
-            total = total + coded.reshape(upto - first, CAP, part) * (their_peak[d] * (1.0 / STEPS_16))
+            total = total + reduced[d, side, first * CAP:upto * CAP].reshape(upto - first, CAP, part)
         back[side, first:upto] = total
         for start in range(first, upto, XS):
             for dx in (2, 1, 3, 0):
@@ -245,8 +229,6 @@
     pl.when(helps)(lambda: wait_some(helping, len(closer), help_sem))
     for swap in swaps:
         swap.wait_send()
-    for d in others:
-        give_peak(d).wait_send()
     for piece in pieces:
         for d in others:
             give(d, piece).wait_send()
@@ -283,10 +265,8 @@
                 pltpu.VMEM((half, CAP, width), jnp.bfloat16),
                 pltpu.VMEM((half, CAP, width), jnp.bfloat16),
                 pltpu.VMEM((half, CAP, width), jnp.bfloat16),
-                pltpu.VMEM((planes - 1, 2, rows, part), jnp.int16),
-                pltpu.VMEM((planes - 1, 2, rows, part), jnp.int16),
-                pltpu.VMEM((planes - 1, CAP, part), jnp.float32),
-                pltpu.VMEM((planes - 1, CAP, part), jnp.float32),
+                pltpu.VMEM((planes - 1, 2, rows, part), jnp.float32),
+                pltpu.VMEM((planes - 1, 2, rows, part), jnp.float32),
                 pltpu.VMEM((2, half, CAP, part), jnp.float32),
                 pltpu.VMEM((groups, CAP, part), jnp.float32),
                 pltpu.SemaphoreType.DMA((7,)),
@@ -297,8 +277,6 @@
                 pltpu.SemaphoreType.DMA((len(CHUNKS),)),
                 pltpu.SemaphoreType.DMA((planes - 1, pieces)),
                 pltpu.SemaphoreType.DMA((planes - 1, pieces)),
-                pltpu.SemaphoreType.DMA((planes - 1,)),
-                pltpu.SemaphoreType.DMA((planes - 1,)),
                 pltpu.SemaphoreType.DMA,
                 pltpu.SemaphoreType.DMA,
             ],

time: 29.2 us -> 30 us (1.027)
  the two profiles are of different devices: /device:TPU:1 before, /device:TPU:96 now
where the time goes in v11:
time: 30 us; the launch traced here: 29.9 us
  Pallas kernels  29.3 us (98%)
  local copies, waits for them, and re-layouts  0.6 us (2%)
    pallas_call x1, Pallas kernels, local(): pl.pallas_call(functools.partial(kernel, groups, shares), out_shape=pltpu...  29.3 us

profile of v11, /device:TPU:96, one launch (start us, length us, event | category | flops | bytes accessed | tf_op | source)
XLA Modules:
  0.0 29.9 jit_solution(12041271194274180992)
XLA Ops:
  0.0 29.3 %experts.1 = bf16[16,128]{1,0:T(8,128)(2,1)S(1)} custom-call(bf16[16,1024]{1,0:T(8,128)(2,1)} %tokens_hbm.1, f32[1,1024]{1,0:T(1,128)} %bitcast.7, s32[2,16]{1,0:T(2,128)} %bitcast.8, f32[2,16]{1,0:T(2,128)} %bitcast.9, bf16[1,448,1024]{2,1,0:T(8,128)(2,1)} %bitcast.5, bf16[1,448,1024]{2,1,0:T(8,128)(2,1)} %bitcast.6, bf16[1,448,1024]{2,1,0:T(8,128)(2,1)} %down_hbm.1), custom_call_target="tpu_custom_call" | custom-call | tf_op jit(solution)/shard_map/experts/pallas_call | solution.py:250
  29.3 0.6 %copy.9 = bf16[16,128]{1,0:T(8,128)(2,1)} copy(bf16[16,128]{1,0:T(8,128)(2,1)S(1)} %experts.1) | data formatting | bytes 8192

commit v12 on v10

--- a/solution.py
+++ b/solution.py
@@ -45,7 +45,7 @@
     tile = 2 * part
 
     barrier = pltpu.get_barrier_semaphore()
-    closer = [(q, dx) for q, dx in rounds if q == 2]
+    closer = [(q, dx) for q, dx in rounds if q == 2 and dx in (2, 1, 3)]
     cross = jnp.logical_and(lower == 0, core == 1).astype(jnp.int32)
     for q, dx in rounds:
         other = 1 - lower - cross if (q, dx) in closer else 1 - lower

time: 29.2 us -> 29 us (level)
  Pallas kernels: 28.5 us -> 28.2 us
where the time goes in v12:
time: 29 us; the launch traced here: 28.8 us
  Pallas kernels  28.2 us (97%)
  local copies, waits for them, and re-layouts  0.6 us (2%)
    pallas_call x1, Pallas kernels, local(): pl.pallas_call(functools.partial(kernel, groups, shares), out_shape=pltpu...  28.2 us
    unnamed x1, local copies, waits for them, and re-layouts  0.6 us

profile of v12, /device:TPU:1, one launch (start us, length us, event | category | flops | bytes accessed | tf_op | source)
XLA Modules:
  0.0 28.8 jit_solution(44159334740061017)
XLA Ops:
  0.0 28.2 %experts.1 = bf16[16,128]{1,0:T(8,128)(2,1)S(1)} custom-call(bf16[16,1024]{1,0:T(8,128)(2,1)} %tokens_hbm.1, f32[1,1024]{1,0:T(1,128)} %bitcast.7, s32[2,16]{1,0:T(2,128)} %bitcast.8, f32[2,16]{1,0:T(2,128)} %bitcast.9, bf16[1,448,1024]{2,1,0:T(8,128)(2,1)} %bitcast.5, bf16[1,448,1024]{2,1,0:T(8,128)(2,1)} %bitcast.6, bf16[1,448,1024]{2,1,0:T(8,128)(2,1)} %down_hbm.1), custom_call_target="tpu_custom_call" | custom-call | tf_op jit(solution)/shard_map/experts/pallas_call | solution.py:268
  28.2 0.6 %copy.9 = bf16[16,128]{1,0:T(8,128)(2,1)} copy(bf16[16,128]{1,0:T(8,128)(2,1)S(1)} %experts.1) | data formatting | bytes 8192

commit v13 on v12

--- a/solution.py
+++ b/solution.py
@@ -10,7 +10,7 @@
 CAP = 8
 XS = 4
 CHUNKS = ((0, 16),)
-PIECES = (((0, 4, 1), (0, 8, 0), (4, 16, 1), (8, 16, 0)),)
+PIECES = (((0, 8, 1), (0, 8, 0), (8, 16, 1), (8, 16, 0)),)
 STEPS = ('c0', 'r0', 'r1', 'r2', 'r3')
 STEPS_16 = 32767.0
 LEAST = 2e-34

time: 29 us -> 29 us (level)
  no operation moved by 1% of the time
where the time goes in v13:
time: 29 us; the launch traced here: 28.9 us
  Pallas kernels  28.3 us (98%)
  local copies, waits for them, and re-layouts  0.6 us (2%)
    pallas_call x1, Pallas kernels, local(): pl.pallas_call(functools.partial(kernel, groups, shares), out_shape=pltpu...  28.3 us
    unnamed x1, local copies, waits for them, and re-layouts  0.6 us

profile of v13, /device:TPU:1, one launch (start us, length us, event | category | flops | bytes accessed | tf_op | source)
XLA Modules:
  0.0 28.9 jit_solution(5309821838308339392)
XLA Ops:
  0.0 28.3 %experts.1 = bf16[16,128]{1,0:T(8,128)(2,1)S(1)} custom-call(bf16[16,1024]{1,0:T(8,128)(2,1)} %tokens_hbm.1, f32[1,1024]{1,0:T(1,128)} %bitcast.7, s32[2,16]{1,0:T(2,128)} %bitcast.8, f32[2,16]{1,0:T(2,128)} %bitcast.9, bf16[1,448,1024]{2,1,0:T(8,128)(2,1)} %bitcast.5, bf16[1,448,1024]{2,1,0:T(8,128)(2,1)} %bitcast.6, bf16[1,448,1024]{2,1,0:T(8,128)(2,1)} %down_hbm.1), custom_call_target="tpu_custom_call" | custom-call | tf_op jit(solution)/shard_map/experts/pallas_call | solution.py:268
  28.3 0.6 %copy.9 = bf16[16,128]{1,0:T(8,128)(2,1)} copy(bf16[16,128]{1,0:T(8,128)(2,1)S(1)} %experts.1) | data formatting | bytes 8192

commit v14 on v12

--- a/solution.py
+++ b/solution.py
@@ -45,15 +45,15 @@
     tile = 2 * part
 
     barrier = pltpu.get_barrier_semaphore()
+    for d in range(1, planes):
+        pl.semaphore_signal(barrier, inc=1, device_id=(ep, 2 * lax.rem(y + d, planes) + core), device_id_type=MESH)
+    pl.semaphore_signal(barrier, inc=1, device_id=(ep, 2 * y + 1 - core), device_id_type=MESH)
+
     closer = [(q, dx) for q, dx in rounds if q == 2 and dx in (2, 1, 3)]
     cross = jnp.logical_and(lower == 0, core == 1).astype(jnp.int32)
     for q, dx in rounds:
         other = 1 - lower - cross if (q, dx) in closer else 1 - lower
         pl.semaphore_signal(barrier, inc=1, device_id=(theirs + near(q, dx), 2 * y + other), device_id_type=MESH)
-    for d in range(1, planes):
-        pl.semaphore_signal(barrier, inc=1, device_id=(ep, 2 * lax.rem(y + d, planes) + core), device_id_type=MESH)
-    pl.semaphore_signal(barrier, inc=1, device_id=(ep, 2 * y + 1 - core), device_id_type=MESH)
-
     pairs = ((tokens_hbm, tokens), (gain_hbm, gain), (routing_hbm, routing), (route_weight_hbm, route_weight),
              (gate_hbm.at[0], gate.at[0:share]), (up_hbm.at[0], up.at[0:share]), (down_hbm.at[0], down.at[0:share]))
     loads = [pltpu.make_async_copy(source, target, load_sem.at[i]) for i, (source, target) in enumerate(pairs)]

time: 29 us -> 29.3 us (1.010)
  Pallas kernels: 28.2 us -> 28.6 us
    pallas_call x1, Pallas kernels: 28.2 us -> 28.6 us  [local(): pl.pallas_call(functools.partial(kernel, groups, shares), out_shape=pltpu...]
where the time goes in v14:
time: 29.3 us; the launch traced here: 29.2 us
  Pallas kernels  28.6 us (98%)
  local copies, waits for them, and re-layouts  0.6 us (2%)
    pallas_call x1, Pallas kernels, local(): pl.pallas_call(functools.partial(kernel, groups, shares), out_shape=pltpu...  28.6 us
    unnamed x1, local copies, waits for them, and re-layouts  0.6 us

profile of v14, /device:TPU:1, one launch (start us, length us, event | category | flops | bytes accessed | tf_op | source)
XLA Modules:
  0.0 29.2 jit_solution(11990236752984642810)
XLA Ops:
  0.0 28.6 %experts.1 = bf16[16,128]{1,0:T(8,128)(2,1)S(1)} custom-call(bf16[16,1024]{1,0:T(8,128)(2,1)} %tokens_hbm.1, f32[1,1024]{1,0:T(1,128)} %bitcast.7, s32[2,16]{1,0:T(2,128)} %bitcast.8, f32[2,16]{1,0:T(2,128)} %bitcast.9, bf16[1,448,1024]{2,1,0:T(8,128)(2,1)} %bitcast.5, bf16[1,448,1024]{2,1,0:T(8,128)(2,1)} %bitcast.6, bf16[1,448,1024]{2,1,0:T(8,128)(2,1)} %down_hbm.1), custom_call_target="tpu_custom_call" | custom-call | tf_op jit(solution)/shard_map/experts/pallas_call | solution.py:268
  28.6 0.6 %copy.9 = bf16[16,128]{1,0:T(8,128)(2,1)} copy(bf16[16,128]{1,0:T(8,128)(2,1)S(1)} %experts.1) | data formatting | bytes 8192
